TPU v7x, 1024 devices: a whole 4x8x16 slice. The times are simulated.
1024 devices in a mesh: sp: 256 (over z, y, core), tp: 4 (over x).
Axes of the slice: x: 4, y: 8, z: 16, core: 2. Of those that a mesh axis runs over, the one named last changes fastest.
Arguments:
- resid: bfloat16 [65536, 2048], P('sp', 'tp'), may hold values from -80 to 80, as said below
- norm_gain: float32 [2, 2048], P(None, 'tp'), may hold values from 0.1 to 1.9
- w_in: bfloat16 [2, 2048, 1024], P(None, 'tp', 'sp'), may hold values from -0.125 to 0.125
- w_pool: bfloat16 [2, 4, 256, 256], P(None, 'tp'), may hold values from -0.375 to 0.375
- pool_scale: float32 [2, 1024], P(None, 'tp'), may hold values from 0.1 to 1.9
- w_out: bfloat16 [2, 1024, 2048], P(None, 'sp', 'tp'), may hold values from -0.1875 to 0.1875
- final_gain: float32 [2048], P('tp'), may hold values from 0.1 to 1.9
Outputs:
- normed: bfloat16 [65536, 2048], P('sp', 'tp')
Inputs may be any that keep to these rules, and one draw needn't show every extreme that they name: `resid`: Real-valued entries of order 0.1 to ten.
All inputs are finite; a program needn't handle non-finite values.
Results may differ from a plain program's by a relative error of at most 0.015.
Values may be sent and summed in bfloat16 or wider, within the bound.
No kernel may reach another device: no remote copies, remote signals or barrier semaphores. Data moves between devices by JAX's collectives and lax.ppermute only.
A program may use at most 32 MiB of HBM per device.

v0:
```python
import jax
import jax.numpy as jnp
from jax import lax
from jax.sharding import PartitionSpec as P

LAYERS = 2


margin = 8
eps = 1e-06


def copy_for_each(value, axis):
    count = lax.axis_size(axis)
    return lax.all_to_all(
        jnp.broadcast_to(value[None], (count, *value.shape)), axis, 0, 0, tiled=True
    )


def taken_together(value, axis):
    return copy_for_each(value, axis).sum(axis=0)


def turned_gather(arrays, axis, dims):
    turned = [jnp.moveaxis(a, dim, 0) for a, dim in zip(arrays, dims)]
    both = jnp.concatenate([t.reshape(len(t), -1) for t in turned], axis=1)
    whole, at, done = (lax.all_gather(both, axis, axis=0, tiled=True), 0, [])
    for t, dim in zip(turned, dims):
        section = whole[:, at : at + t[0].size].reshape(-1, *t.shape[1:])
        done.append(jnp.moveaxis(section, 0, dim))
        at += t[0].size
    return tuple(done)


def in_blocks(value, dim, count):
    shape = value.shape
    pieces = value.reshape(*shape[:dim], count, shape[dim] // count, *shape[dim + 1 :])
    return jnp.moveaxis(pieces, dim, 0)


def sum_at_owner(value, axis, dim):
    count = lax.axis_size(axis)
    pieces = lax.all_to_all(in_blocks(value, dim, count), axis, 0, 0, tiled=True)
    return jnp.sum(pieces.astype(jnp.float32), axis=0)


def padded_2(value, sides, width):
    for axis, dim in sides:
        count, length = (lax.axis_size(axis), value.shape[dim])
        up = [(i, (i + 1) % count) for i in range(count - 1)]
        down = [(j, i) for i, j in up]
        last = lax.slice_in_dim(value, length - width, length, axis=dim)
        initial = lax.slice_in_dim(value, 0, width, axis=dim)
        before = lax.ppermute(last, axis, up)
        after = lax.ppermute(initial, axis, down)
        value = jnp.concatenate([before, value, after], axis=dim)
    return value


def laid_out(pieces, dim):
    shape = list(pieces.shape[1:])
    shape[dim] *= pieces.shape[0]
    return jnp.moveaxis(pieces, 0, dim).reshape(shape)


def gather_directly(value, axis, dim):
    pieces = copy_for_each(value, axis)
    return laid_out(pieces, dim)


def nested_sums(padded, count_rows):
    total = padded[margin - 1 : margin - 1 + count_rows] + padded[margin : margin + count_rows]
    sums = [total]
    for level in range(1, 4):
        half = 2**level
        for offset in range(half // 2 + 1, half + 1):
            total = total + padded[margin - offset : margin - offset + count_rows]
        for offset in range(half // 2, half):
            total = total + padded[margin + offset : margin + offset + count_rows]
        sums.append(total)
    return sums


def window_count(where, seq_len, level):
    left = 2**level
    right = 2**level - 1
    upper = jnp.clip(where + right + 1, 0, seq_len)
    lower = jnp.clip(where - left, 0, seq_len)
    return (upper - lower).astype(jnp.float32)


def scaled(xf, gain, width):
    squares = taken_together(jnp.sum(xf * xf, axis=1), "tp")
    return (xf * lax.rsqrt(squares / width + eps)[:, None] * gain[None, :]).astype(jnp.bfloat16)


def shards(resid, norm_gain, w_in, w_pool, pool_scale, w_out, final_gain):
    tok_rows = resid.shape[0]
    blocks_tp = lax.axis_size("tp")
    width = blocks_tp * resid.shape[1]
    channels = w_pool.shape[1] * w_pool.shape[2]
    groups_here = w_pool.shape[1]
    group_width = w_pool.shape[2]
    seq_len = tok_rows * lax.axis_size("sp")
    where = lax.axis_index("sp") * tok_rows + jnp.arange(tok_rows, dtype=jnp.int32)
    group_ids = (
        lax.axis_index("tp") * groups_here + jnp.arange(channels, dtype=jnp.int32) // group_width
    )
    all_in, all_out = turned_gather((w_in, w_out), "sp", (2, 1))
    xf = resid.astype(jnp.float32)
    for layer in range(LAYERS):
        own_hidden = scaled(xf, norm_gain[layer], width)
        in_block = all_in[layer]
        partial_value = jnp.dot(own_hidden, in_block, preferred_element_type=jnp.float32).astype(
            jnp.bfloat16
        )
        upward = sum_at_owner(partial_value, "tp", 1).astype(jnp.bfloat16)
        padded = padded_2(upward, (("sp", 0),), margin).astype(jnp.float32)
        sums = nested_sums(padded, tok_rows)
        wsum = sums[0]
        counted = jnp.broadcast_to(window_count(where, seq_len, 0)[:, None], (tok_rows, channels))
        for level in range(1, 4):
            chosen = (group_ids == level)[None, :]
            wsum = jnp.where(chosen, sums[level], wsum)
            counted = jnp.where(chosen, window_count(where, seq_len, level)[:, None], counted)
        pooled = (wsum / counted - upward.astype(jnp.float32)).astype(jnp.bfloat16)
        mapped = jnp.einsum(
            "tgc,gcd->tgd",
            pooled.reshape(tok_rows, groups_here, group_width),
            w_pool[layer],
            preferred_element_type=jnp.float32,
        )
        mixed = (mapped.reshape(tok_rows, channels) * pool_scale[layer][None, :]).astype(
            jnp.bfloat16
        )
        mixed_all = gather_directly(mixed, "tp", 1)
        output = jnp.dot(mixed_all, all_out[layer], preferred_element_type=jnp.float32)
        stored = (xf + output).astype(jnp.bfloat16)
        stored = lax.optimization_barrier(stored)
        xf = stored.astype(jnp.float32)
    return scaled(xf, final_gain, width)


def solution(mesh):
    placed = (
        P("sp", "tp"),
        P(None, "tp"),
        P(None, "tp", "sp"),
        P(None, "tp", None, None),
        P(None, "tp"),
        P(None, "sp", "tp"),
        P("tp"),
    )
    return jax.shard_map(
        shards, mesh=mesh, in_specs=placed, out_specs=P("sp", "tp"), check_vma=False
    )
```

profile of v0, /device:TPU:25, one launch (start us, length us, event | category | flops | bytes accessed | tf_op | source)
XLA Modules:
  0.0 280.6 jit_solution(11613713160797136765)
XLA Ops:
  6.5 0.0 all-gather.3.cloned.1.call-start
  6.5 1.3 maximum_bitcast_fusion
  7.9 0.0 all-gather.3.cloned.1.call-update
  7.9 1.1 fusion.7
  9.0 0.6 broadcast_in_dim.132
  9.6 4.0 %all-to-all-start = ((f32[4,1,256]{2,1,0:T(1,128)}), f32[4,1,256]{2,1,0:T(1,128)S(1)}, u32[]{:S(2)}, u32[]{:S(2)}) async-start(f32[4,1,256]{2,1,0:T(1,128)} %broadcast_in_dim.132), calls=%async_computation | async-start | bytes 8192 | tf_op jit(solution)/shard_map/all_to_all | solution.py:15
  13.6 0.8 fusion.37
  14.4 3.4 %all-to-all-done = f32[4,1,256]{2,1,0:T(1,128)S(1)} async-done(((f32[4,1,256]{2,1,0:T(1,128)}), f32[4,1,256]{2,1,0:T(1,128)S(1)}, u32[]{:S(2)}, u32[]{:S(2)}) %all-to-all-start) | async-done | bytes 4128 | tf_op jit(solution)/shard_map/all_to_all | solution.py:15
  17.8 150.5 %all-gather.3.cloned.1.call-done = bf16[256,4,2048]{2,1,0:T(4,128)(2,1)} async-done(((bf16[1,4,2048]{2,1,0:T(4,128)(2,1)}), bf16[256,4,2048]{2,1,0:T(4,128)(2,1)}) %all-gather.3.cloned.1.call-update) | async-done | bytes 4194320 | tf_op jit(solution)/shard_map/all_gather | solution.py:27
  168.3 6.9 %reshape.186 = bf16[1024,2048]{1,0:T(8,128)(2,1)} reshape(bf16[256,4,2048]{2,1,0:T(4,128)(2,1)} %all-gather.3.cloned.1.call-done) | data formatting | bytes 8388608
  175.2 4.0 %fusion.34 = (bf16[1024,1024]{1,0:T(8,128)(2,1)S(1)}, bf16[1024,1024]{1,0:T(8,128)(2,1)}) fusion(bf16[1024,2048]{1,0:T(8,128)(2,1)} %reshape.186), kind=kLoop, calls=%fused_computation.97 | loop fusion | bytes 8388608 | tf_op jit(solution)/shard_map/slice | solution.py:29
  179.2 4.0 %copy.43 = bf16[1024,1024]{0,1:T(8,128)(2,1)} copy(bf16[1024,1024]{1,0:T(8,128)(2,1)} %get-tuple-element.6) | data formatting | bytes 4194304 | tf_op jit(solution)/shard_map/reshape | solution.py:29
  183.2 0.0 copy-done.2
  183.2 1.7 convolution_convert_fusion.1
  184.9 0.8 copy.52
  185.7 4.0 %all-to-all-start.1 = ((bf16[4,256,256]{2,1,0:T(8,128)(2,1)}), bf16[4,256,256]{2,1,0:T(8,128)(2,1)S(1)}, u32[]{:S(2)}, u32[]{:S(2)}) async-start(bf16[4,256,256]{2,1,0:T(8,128)(2,1)} %bitcast.59), calls=%async_computation.1 | async-start | bytes 1048576 | tf_op jit(solution)/shard_map/all_to_all | solution.py:43
  189.7 0.0 copy-done.4
  189.7 9.0 %all-to-all-done.1 = bf16[4,256,256]{2,1,0:T(8,128)(2,1)S(1)} async-done(((bf16[4,256,256]{2,1,0:T(8,128)(2,1)}), bf16[4,256,256]{2,1,0:T(8,128)(2,1)S(1)}, u32[]{:S(2)}, u32[]{:S(2)}) %all-to-all-start.1) | async-done | bytes 524320 | tf_op jit(solution)/shard_map/all_to_all | solution.py:43
  198.7 0.1 reduce_sum.80
  198.8 4.6 %collective-permute-start = (bf16[8,256]{1,0:T(8,128)(2,1)S(1)}, bf16[8,256]{1,0:T(8,128)(2,1)S(1)}, u32[]{:S(2)}, u32[]{:S(2)}) collective-permute-start(bf16[8,256]{1,0:T(8,128)(2,1)S(1)} %get-tuple-element.9), channel_id=1, source_target_pairs={{0,4},{4,8},{8,12},{12,16},{16,20},{20,24},{24,28},{28,32},{32,36}... | collective-permute-start | bytes 12296 | tf_op jit(solution)/shard_map/ppermute | solution.py:54
  203.4 1.9 collective-permute-start.1
  205.4 0.0 collective-permute-done
  205.4 4.2 %collective-permute-done.1 = bf16[8,256]{1,0:T(8,128)(2,1)S(1)} collective-permute-done((bf16[8,256]{1,0:T(8,128)(2,1)S(1)}, bf16[8,256]{1,0:T(8,128)(2,1)S(1)}, u32[]{:S(2)}, u32[]{:S(2)}) %collective-permute-start.1) | collective-permute-done | bytes 4128 | tf_op jit(solution)/shard_map/ppermute | solution.py:55
  209.6 1.5 fusion.2
  211.1 0.1 copy.35
  211.2 0.8 broadcast_in_dim.139
  212.1 3.5 %all-to-all-start.2 = ((bf16[4,256,256]{1,2,0:T(8,128)(2,1)}), bf16[4,256,256]{1,2,0:T(8,128)(2,1)S(1)}, u32[]{:S(2)}, u32[]{:S(2)}) async-start(bf16[4,256,256]{1,2,0:T(8,128)(2,1)} %broadcast_in_dim.139), calls=%async_computation.2 | async-start | bytes 1048576 | tf_op jit(solution)/shard_map/all_to_all | solution.py:15
  215.5 2.6 copy.36
  218.1 5.1 %all-to-all-done.2 = bf16[4,256,256]{1,2,0:T(8,128)(2,1)S(1)} async-done(((bf16[4,256,256]{1,2,0:T(8,128)(2,1)}), bf16[4,256,256]{1,2,0:T(8,128)(2,1)S(1)}, u32[]{:S(2)}, u32[]{:S(2)}) %all-to-all-start.2) | async-done | bytes 524320 | tf_op jit(solution)/shard_map/all_to_all | solution.py:15
  223.2 1.7 fusion
  225.0 0.1 fusion.10
  225.1 6.5 %all_to_all.38 = f32[4,1,256]{2,1,0:T(1,128)S(1)} all-to-all(f32[4,1,256]{2,1,0:T(1,128)S(1)} %broadcast_in_dim.140), channel_id=1, replica_groups=mesh['sp'=256,'tp'=4] {'tp'}, dimensions={0} | all-to-all | bytes 8192 | tf_op jit(solution)/shard_map/all_to_all | solution.py:15
  231.6 0.5 convolution_convert_fusion
  232.1 0.0 copy-start.5
  232.2 12.3 %all_to_all.39 = bf16[4,256,256]{2,1,0:T(8,128)(2,1)S(1)} all-to-all(bf16[4,256,256]{2,1,0:T(8,128)(2,1)S(1)} %bitcast.64), channel_id=1, replica_groups=mesh['sp'=256,'tp'=4] {'tp'}, dimensions={0} | all-to-all | bytes 1048576 | tf_op jit(solution)/shard_map/all_to_all | solution.py:43
  244.5 0.1 reduce_sum.83
  244.6 3.2 %collective-permute-start.2 = (bf16[8,256]{1,0:T(8,128)(2,1)S(1)}, bf16[8,256]{1,0:T(8,128)(2,1)S(1)}, u32[]{:S(2)}, u32[]{:S(2)}) collective-permute-start(bf16[8,256]{1,0:T(8,128)(2,1)S(1)} %get-tuple-element.7), channel_id=1, source_target_pairs={{0,4},{4,8},{8,12},{12,16},{16,20},{20,24},{24,28},{28,32},{32,36}... | collective-permute-start | bytes 12296 | tf_op jit(solution)/shard_map/ppermute | solution.py:54
  247.7 1.9 collective-permute-start.3
  249.6 0.0 collective-permute-done.2
  249.7 4.2 %collective-permute-done.3 = bf16[8,256]{1,0:T(8,128)(2,1)S(1)} collective-permute-done((bf16[8,256]{1,0:T(8,128)(2,1)S(1)}, bf16[8,256]{1,0:T(8,128)(2,1)S(1)}, u32[]{:S(2)}, u32[]{:S(2)}) %collective-permute-start.3) | collective-permute-done | bytes 4128 | tf_op jit(solution)/shard_map/ppermute | solution.py:55
  253.9 0.6 fusion.3
  254.5 0.1 copy.40
  254.7 0.0 copy-start.3
  254.7 10.9 %all_to_all.40 = bf16[4,256,256]{1,2,0:T(8,128)(2,1)S(1)} all-to-all(bf16[4,256,256]{1,2,0:T(8,128)(2,1)S(1)} %broadcast_in_dim.141), channel_id=1, replica_groups=mesh['sp'=256,'tp'=4] {'tp'}, dimensions={0} | all-to-all | bytes 1048576 | tf_op jit(solution)/shard_map/all_to_all | solution.py:15
  265.6 0.5 fusion.1
  266.1 0.1 fusion.4
  266.2 6.7 %all_to_all.41 = f32[4,1,256]{2,1,0:T(1,128)S(1)} all-to-all(f32[4,1,256]{2,1,0:T(1,128)S(1)} %broadcast_in_dim.142), channel_id=1, replica_groups=mesh['sp'=256,'tp'=4] {'tp'}, dimensions={0} | all-to-all | bytes 8192 | tf_op jit(solution)/shard_map/all_to_all | solution.py:15
  272.9 0.8 fusion.6
  (27 shorter events, 0.3 us)
Async XLA Ops:
  6.5 161.7 %all-gather.3.cloned.1.call-start = ((), (), s32[]{:S(2)}) async-start(), calls=%async_computation.7 | async-start | bytes 4210688 | tf_op jit(solution)/shard_map/all_gather | solution.py:27
  9.6 8.2 %all-to-all-start = ((f32[4,1,256]{2,1,0:T(1,128)}), f32[4,1,256]{2,1,0:T(1,128)S(1)}, u32[]{:S(2)}, u32[]{:S(2)}) async-start(f32[4,1,256]{2,1,0:T(1,128)} %broadcast_in_dim.132), calls=%async_computation | async-start | bytes 8192 | tf_op jit(solution)/shard_map/all_to_all | solution.py:15
  179.2 4.0 %copy-start.2 = (bf16[256,512]{1,0:T(8,128)(2,1)S(1)}, bf16[256,512]{1,0:T(8,128)(2,1)}, u32[]{:S(2)}) copy-start(bf16[256,512]{1,0:T(8,128)(2,1)} %param.7) | copy-start | bytes 786436
  183.2 6.6 %copy-start.4 = (f32[2,256]{1,0:T(2,128)S(1)}, f32[2,256]{1,0:T(2,128)}, u32[]{:S(2)}) copy-start(f32[2,256]{1,0:T(2,128)} %param.11) | copy-start | bytes 6148
  185.7 13.0 %all-to-all-start.1 = ((bf16[4,256,256]{2,1,0:T(8,128)(2,1)}), bf16[4,256,256]{2,1,0:T(8,128)(2,1)S(1)}, u32[]{:S(2)}, u32[]{:S(2)}) async-start(bf16[4,256,256]{2,1,0:T(8,128)(2,1)} %bitcast.59), calls=%async_computation.1 | async-start | bytes 1048576 | tf_op jit(solution)/shard_map/all_to_all | solution.py:43
  198.8 6.6 %collective-permute-start = (bf16[8,256]{1,0:T(8,128)(2,1)S(1)}, bf16[8,256]{1,0:T(8,128)(2,1)S(1)}, u32[]{:S(2)}, u32[]{:S(2)}) collective-permute-start(bf16[8,256]{1,0:T(8,128)(2,1)S(1)} %get-tuple-element.9), channel_id=1, source_target_pairs={{0,4},{4,8},{8,12},{12,16},{16,20},{20,24},{24,28},{28,32},{32,36}... | collective-permute-start | bytes 12296 | tf_op jit(solution)/shard_map/ppermute | solution.py:54
  203.4 6.1 %collective-permute-start.1 = (bf16[8,256]{1,0:T(8,128)(2,1)S(1)}, bf16[8,256]{1,0:T(8,128)(2,1)S(1)}, u32[]{:S(2)}, u32[]{:S(2)}) collective-permute-start(bf16[8,256]{1,0:T(8,128)(2,1)S(1)} %get-tuple-element.10), channel_id=1, source_target_pairs={{4,0},{8,4},{12,8},{16,12},{20,16},{24,20},{28,24},{32,28},{36,32}... | collective-permute-start | bytes 12296 | tf_op jit(solution)/shard_map/ppermute | solution.py:55
  212.1 11.2 %all-to-all-start.2 = ((bf16[4,256,256]{1,2,0:T(8,128)(2,1)}), bf16[4,256,256]{1,2,0:T(8,128)(2,1)S(1)}, u32[]{:S(2)}, u32[]{:S(2)}) async-start(bf16[4,256,256]{1,2,0:T(8,128)(2,1)} %broadcast_in_dim.139), calls=%async_computation.2 | async-start | bytes 1048576 | tf_op jit(solution)/shard_map/all_to_all | solution.py:15
  218.1 13.5 %copy-start = (bf16[1024,1024]{0,1:T(8,128)(2,1)S(1)}, bf16[1024,1024]{0,1:T(8,128)(2,1)}, u32[]{:S(2)}) copy-start(bf16[1024,1024]{0,1:T(8,128)(2,1)} %copy.43) | copy-start | bytes 6291460
  232.1 21.7 %copy-start.5 = (bf16[2,1,256,256]{3,2,1,0:T(8,128)(2,1)S(1)}, bf16[2,1,256,256]{3,2,1,0:T(8,128)(2,1)}, u32[]{:S(2)}) copy-start(bf16[2,1,256,256]{3,2,1,0:T(8,128)(2,1)} %param.10) | copy-start | bytes 786436
  244.6 5.1 %collective-permute-start.2 = (bf16[8,256]{1,0:T(8,128)(2,1)S(1)}, bf16[8,256]{1,0:T(8,128)(2,1)S(1)}, u32[]{:S(2)}, u32[]{:S(2)}) collective-permute-start(bf16[8,256]{1,0:T(8,128)(2,1)S(1)} %get-tuple-element.7), channel_id=1, source_target_pairs={{0,4},{4,8},{8,12},{12,16},{16,20},{20,24},{24,28},{28,32},{32,36}... | collective-permute-start | bytes 12296 | tf_op jit(solution)/shard_map/ppermute | solution.py:54
  247.7 6.1 %collective-permute-start.3 = (bf16[8,256]{1,0:T(8,128)(2,1)S(1)}, bf16[8,256]{1,0:T(8,128)(2,1)S(1)}, u32[]{:S(2)}, u32[]{:S(2)}) collective-permute-start(bf16[8,256]{1,0:T(8,128)(2,1)S(1)} %get-tuple-element.8), channel_id=1, source_target_pairs={{4,0},{8,4},{12,8},{16,12},{20,16},{24,20},{28,24},{32,28},{36,32}... | collective-permute-start | bytes 12296 | tf_op jit(solution)/shard_map/ppermute | solution.py:55
  253.9 11.7 %copy-start.1 = (bf16[1024,1024]{0,1:T(8,128)(2,1)S(1)}, bf16[1024,1024]{0,1:T(8,128)(2,1)}, u32[]{:S(2)}) copy-start(bf16[1024,1024]{0,1:T(8,128)(2,1)} %copy.36) | copy-start | bytes 6291460
  254.7 18.2 %copy-start.3 = (f32[512]{0:T(512)S(1)}, f32[512]{0:T(512)}, u32[]{:S(2)}) copy-start(f32[512]{0:T(512)} %param.13) | copy-start | bytes 6148
Sparse Core Ops, SparseCore 0:
  11.6 156.6 all-gather.2
where the time goes:
time: 281 us
  waiting for transfers between devices  176 us (63%)
  blocking collectives  36.3 us (13%)
  starting transfers between devices  23.1 us (8%)
  local copies, waits for them, and re-layouts  20.8 us (7%)
  between operations  13.6 us (5%)
  matrix products  6.57 us (2%)
  other arithmetic  3.84 us (1%)
    all_gather x1, waiting for transfers between devices, turned_gather(): whole, at, done = (lax.all_gather(both, axis, axis=0, tiled=True), 0, [])  151 us
    all_to_all x3, blocking collectives, copy_for_each(): lax.all_to_all(jnp.broadcast_to(value[None], (count, *value.shape)), axis...  24 us
    all_to_all x1, blocking collectives, sum_at_owner(): lax.all_to_all(in_blocks(value, dim, count), axis, 0, 0, tiled=True)  12.3 us
    all_to_all x1, waiting for transfers between devices, sum_at_owner(): lax.all_to_all(in_blocks(value, dim, count), axis, 0, 0, tiled=True)  8.96 us
    all_to_all x2, waiting for transfers between devices, copy_for_each(): lax.all_to_all(jnp.broadcast_to(value[None], (count, *value.shape)), axis...  8.49 us
    ppermute x2, waiting for transfers between devices, padded_2(): after = lax.ppermute(initial, axis, down)  8.38 us
    ppermute x2, starting transfers between devices, padded_2(): before = lax.ppermute(last, axis, up)  7.78 us
    all_to_all x2, starting transfers between devices, copy_for_each(): lax.all_to_all(jnp.broadcast_to(value[None], (count, *value.shape)), axis...  7.48 us
  transfers between devices with their start and end apart: 8, of which 6 were waited for; matrix products, arithmetic and copies ran while one was open for 2% of the time, Pallas kernels for 0%

commit v1 on v0

v1 whole, which is shorter than its diff:
```python
import functools

import jax
import jax.numpy as jnp
from jax import lax
from jax.experimental import pallas as pl
from jax.experimental.pallas import tpu as pltpu
from jax.sharding import PartitionSpec as P


EPS = 1e-06
MARGIN = 8
Y, C = 8, 2
BF, F32 = jnp.bfloat16, jnp.float32
LIMIT = 16 * 2**20
ROWS = 16


def order_matrix(core, base, size):
    pos = lax.broadcasted_iota(jnp.int32, (size, size), 0)
    nat = lax.broadcasted_iota(jnp.int32, (size, size), 1)
    half = Y * 16
    y = (base + ((pos & (half - 1)) >> 4)) & (Y - 1)
    c = core ^ jnp.where(pos >= half, 1, 0)
    zr, r = (pos >> 2) & 3, pos & 3
    where = zr * (Y * C * 4) + y * (C * 4) + c * 4 + r
    return jnp.where(where == nat, 1.0, 0.0).astype(BF)


def dot_nt(a, b):
    return lax.dot_general(a, b, (((1,), (1,)), ((), ())), preferred_element_type=F32)


def dot_nn(a, b):
    return jnp.dot(a, b, preferred_element_type=F32)


def square_rows(xf):
    sq = xf * xf
    hi = sq.astype(BF)
    lo = (sq - hi.astype(F32)).astype(BF)
    ones = jnp.ones((ROWS, xf.shape[1]), BF)
    return dot_nt(ones, hi) + dot_nt(ones, lo)


def to_column(row, rows):
    return jnp.transpose(jnp.broadcast_to(row, (128, rows)))


def group_rows(picks, g):
    parts = []
    for ref, q in picks:
        block = ref[:, g] if q is None else ref[:, q, g]
        n, rows, d = block.shape
        parts.append(block.reshape(n * rows, d))
    return jnp.concatenate(parts, axis=0)


def project(xf, gain, picks, outs, first_group):
    rows = xf.shape[0]
    xs = (xf * gain).astype(BF)
    first, last = square_rows(xf[:256]), square_rows(xf[rows - 256 :])
    f_hi, l_hi = first.astype(BF).astype(F32), last.astype(BF).astype(F32)
    row = lax.broadcasted_iota(jnp.int32, first.shape, 0)
    extra = jnp.where(
        row == 0,
        f_hi,
        jnp.where(row == 1, first - f_hi, jnp.where(row == 2, l_hi, jnp.where(row == 3, last - l_hi, 0.0))),
    ).astype(BF)
    for d, out in enumerate(outs):
        g = (first_group + d) & (len(outs) - 1)
        out[:rows] = dot_nt(xs, group_rows(picks, g)).astype(BF)
        out[rows:] = extra


def first_kernel(info, prev, own, after, gain, in_own, in_other, *outs):
    xf = jnp.concatenate([prev[...].astype(F32), own[...].astype(F32), after[...].astype(F32)], axis=0)
    project(xf, gain[0:1], ((in_own, None), (in_other, None)), outs, info[0])


def pool_kernel(seq_len, width, halo, layer, copies, info, wp, scale, *refs):
    recv, out = refs[:-1], refs[-1]
    if len(recv) == 1:
        recv = [recv[0].at[k] for k in range(recv[0].shape[0])]
    size = recv[0].shape[1]
    rows = recv[0].shape[0] - ROWS
    keep = rows - 2 * MARGIN
    g, core, tok0 = info[0], info[1], info[2]
    total = recv[0][:rows].astype(F32)
    extra = recv[0][rows:].astype(F32)
    for ref in recv[1:]:
        total = total + ref[:rows].astype(F32)
        extra = extra + ref[rows:].astype(F32)
    first = to_column(extra[0:1] + extra[1:2], 256)
    last = to_column(extra[2:3] + extra[3:4], 256)
    ss = jnp.concatenate([first, last[512 - rows :]], axis=0) if rows > 256 else first
    r = lax.rsqrt(ss / width + EPS)
    uf = total * jnp.concatenate([r, r], axis=1)
    at = tok0 - halo + lax.broadcasted_iota(jnp.int32, (rows, size), 0)
    uf = jnp.where((at >= 0) & (at < seq_len), uf, 0.0)
    u = uf.astype(BF)
    left = jnp.left_shift(1, g)
    d = (
        lax.broadcasted_iota(jnp.int32, (keep, rows), 1)
        - lax.broadcasted_iota(jnp.int32, (keep, rows), 0)
        - MARGIN
    )
    band = jnp.where((d >= -left) & (d < left), 1.0, 0.0).astype(BF)
    wsum = dot_nn(band, u)
    here = tok0 - halo + MARGIN + lax.broadcasted_iota(jnp.int32, (keep, size), 0)
    upper = jnp.clip(here + left, 0, seq_len)
    lower = jnp.clip(here - left, 0, seq_len)
    count = jnp.maximum(upper - lower, 1).astype(F32)
    pooled = (wsum / count - u.astype(F32)[MARGIN : MARGIN + keep]).astype(BF)
    order = order_matrix(core, 0, size)
    inner = dot_nn(order, wp[layer, 0]).astype(BF)
    mixed = (dot_nn(pooled, inner) * scale[layer : layer + 1]).astype(BF)
    mixed = dot_nt(mixed, order).astype(BF)
    if copies is None:
        out[...] = mixed
    else:
        for k in range(copies):
            out[k] = mixed


def added(xf, mixed, picks):
    total = xf
    for g in range(mixed.shape[0]):
        total = total + dot_nn(mixed[g], group_rows(picks, g))
    return total.astype(BF)


def middle_kernel(out_q, in_q, prev, own, after, mixed, gain, w_own, w_other, x_out, pay):
    xf = jnp.concatenate(
        [prev[...].astype(F32)[8:], own[...].astype(F32), after[...].astype(F32)[:8]], axis=0
    )
    x = added(xf, mixed, ((w_own, out_q), (w_other, out_q)))
    x_out[...] = x
    outs = [pay.at[k] for k in range(pay.shape[0])]
    project(x.astype(F32), gain[1:2], ((w_own, in_q), (w_other, in_q)), outs, 0)


def last_kernel(out_q, x_in, mixed, w_own, w_other, x_out, squares):
    rows = mixed.shape[1]
    xf = x_in[...].astype(F32)[MARGIN : MARGIN + rows]
    x = added(xf, mixed, ((w_own, out_q), (w_other, out_q)))
    x_out[...] = x
    sums = square_rows(x.astype(F32))[:8]
    for k in range(squares.shape[0]):
        squares[k] = sums


def norm_kernel(width, x_in, squares, gain, out):
    total = squares[0, 0:1]
    for k in range(1, squares.shape[0]):
        total = total + squares[k, 0:1]
    rows, d = x_in.shape
    r = lax.rsqrt(to_column(total, rows) / width + EPS)
    r = jnp.concatenate([r] * (d // 128), axis=1)
    out[...] = (x_in[...].astype(F32) * r * gain[...]).astype(BF)


def call(kernel, shapes, *args, smem=0):
    spaces = [pltpu.SMEM if i < smem else pltpu.VMEM for i in range(len(args))]
    specs = [pl.BlockSpec(memory_space=space) for space in spaces]
    held = [
        a if space is pltpu.SMEM else pltpu.with_memory_space_constraint(a, space)
        for a, space in zip(args, spaces)
    ]
    params = pltpu.CompilerParams(vmem_limit_bytes=LIMIT)
    return pl.pallas_call(kernel, out_shape=shapes, in_specs=specs, compiler_params=params)(*held)


def to_all(value, axis, groups=None, count=None):
    count = lax.axis_size(axis) if count is None else count
    return lax.all_to_all(
        jnp.broadcast_to(value[None], (count, *value.shape)), axis, 0, 0, axis_index_groups=groups
    )


def shards(resid, norm_gain, w_in, w_pool, pool_scale, w_out, final_gain):
    tok = resid.shape[0]
    block = resid.shape[1]
    n_sp, n_tp = lax.axis_size("sp"), lax.axis_size("tp")
    width = n_tp * block
    seq_len = tok * n_sp
    nz = n_sp // (Y * C)
    size = w_pool.shape[2]
    sp, tp = lax.axis_index("sp"), lax.axis_index("tp")
    at = lambda z, y, c: ((z % nz) * Y + (y % Y)) * C + c
    places = [(z, y, c) for z in range(nz) for y in range(Y) for c in range(C)]
    z_rings = [[at(z, y, c) for z in range(nz)] for y in range(Y) for c in range(C)]
    y_rings = [[at(z, y, c) for y in range(Y)] for z in range(nz) for c in range(C)]
    swap = [(at(z, y, c), at(z, y, 1 - c)) for z, y, c in places]
    send_across = lambda v: lax.ppermute(v, "sp", swap)

    before = lax.ppermute(resid[tok - 2 * MARGIN :], "sp", [(i, i + 1) for i in range(n_sp - 1)])
    after = lax.ppermute(resid[: 2 * MARGIN], "sp", [(i + 1, i) for i in range(n_sp - 1)])

    turned = jnp.swapaxes(w_in, 1, 2)
    mine = jnp.stack([turned[0], w_out[0], turned[1], w_out[1]])
    along_z = to_all(mine, "sp", z_rings, nz)
    along_z = jnp.swapaxes(along_z, 0, 1).reshape(4, n_tp, nz // n_tp * 4, block)
    early, late, before, after = lax.optimization_barrier(
        (along_z[0], along_z[1:], before, after)
    )
    in_own = to_all(early, "sp", y_rings, Y)
    in_other = send_across(in_own)
    late, in_own = lax.optimization_barrier((late, in_own))
    own = to_all(late, "sp", y_rings, Y)
    other = send_across(own)

    info = jnp.stack([tp, sp & (C - 1), sp * tok]).astype(jnp.int32)
    wide, mid = tok + 4 * MARGIN, tok + 2 * MARGIN
    exchange = lambda v: lax.all_to_all(v, "tp", 0, 0, tiled=True)

    pay = call(
        first_kernel,
        [jax.ShapeDtypeStruct((wide + ROWS, size), BF)] * n_tp,
        info, before, resid, after, norm_gain, in_own, in_other, smem=1,
    )
    recv = [pay[0]]
    for d in (2, 1, 3):
        recv.append(lax.ppermute(pay[d], "tp", [(i, (i + d) % n_tp) for i in range(n_tp)]))
    mixed = call(
        functools.partial(pool_kernel, seq_len, width, 2 * MARGIN, 0, None),
        jax.ShapeDtypeStruct((mid, size), BF),
        info, w_pool, pool_scale, *recv, smem=1,
    )
    mixed = lax.all_gather(mixed, "tp")
    x, pay = call(
        functools.partial(middle_kernel, 0, 1),
        (
            jax.ShapeDtypeStruct((mid, block), BF),
            jax.ShapeDtypeStruct((n_tp, mid + ROWS, size), BF),
        ),
        before, resid, after, mixed, norm_gain, own, other,
    )
    recv = exchange(pay)
    mixed = call(
        functools.partial(pool_kernel, seq_len, width, MARGIN, 1, n_tp),
        jax.ShapeDtypeStruct((n_tp, tok, size), BF),
        info, w_pool, pool_scale, recv, smem=1,
    )
    mixed = exchange(mixed)
    x, squares = call(
        functools.partial(last_kernel, 2),
        (jax.ShapeDtypeStruct((tok, block), BF), jax.ShapeDtypeStruct((n_tp, 8, tok), F32)),
        x, mixed, own, other,
    )
    squares = exchange(squares)
    return call(
        functools.partial(norm_kernel, width),
        jax.ShapeDtypeStruct((tok, block), BF),
        x, squares, final_gain[None],
    )


def solution(mesh):
    placed = (
        P("sp", "tp"),
        P(None, "tp"),
        P(None, "tp", "sp"),
        P(None, "tp", None, None),
        P(None, "tp"),
        P(None, "sp", "tp"),
        P("tp"),
    )

    return jax.shard_map(
        shards, mesh=mesh, in_specs=placed, out_specs=P("sp", "tp"), check_vma=False
    )
```

time: 281 us -> 178 us (0.63)
  the two profiles are of different devices: /device:TPU:25 before, /device:TPU:64 now
where the time goes in v1:
time: 178 us; the launch traced here: 177 us
  blocking collectives  109 us (61%)
  starting transfers between devices  40.7 us (23%)
  waiting for transfers between devices  16.2 us (9%)
  Pallas kernels  7.43 us (4%)
  local copies, waits for them, and re-layouts  3.74 us (2%)
    all_to_all x2, blocking collectives, to_all(): lax.all_to_all(jnp.broadcast_to(value[None], (count, *value.shape)), axis...  64.5 us
    all_to_all x3, blocking collectives, shards(): exchange = lambda v: lax.all_to_all(v, 'tp', 0, 0, tiled=True)  31 us
    all_to_all x1, starting transfers between devices, to_all(): lax.all_to_all(jnp.broadcast_to(value[None], (count, *value.shape)), axis...  18.4 us
    all_gather x1, blocking collectives, shards(): mixed = lax.all_gather(mixed, 'tp')  13.3 us
    ppermute x3, starting transfers between devices, shards(): lax.ppermute(pay[d], 'tp', [(i, (i + d) % n_tp) for i in range(n_tp)])  12 us
    all_to_all x1, waiting for transfers between devices, to_all(): lax.all_to_all(jnp.broadcast_to(value[None], (count, *value.shape)), axis...  11.2 us
    pallas_call x6, Pallas kernels, call(): pl.pallas_call(kernel, out_shape=shapes, in_specs=specs, compiler_params=...  7.43 us
    ppermute x2, starting transfers between devices, shards(): send_across = lambda v: lax.ppermute(v, 'sp', swap)  4.32 us
  transfers between devices with their start and end apart: 8, of which 4 were waited for; matrix products, arithmetic and copies ran while one was open for 1% of the time, Pallas kernels for 2%

profile of v1, /device:TPU:64, one launch (start us, length us, event | category | flops | bytes accessed | tf_op | source)
XLA Modules:
  0.0 177.2 jit_solution(8952580102830374586)
XLA Ops:
  0.0 0.7 fusion.1
  0.8 0.8 broadcast_in_dim.8
  1.6 18.4 %all-to-all-start = ((bf16[16,4,4,512]{3,2,1,0:T(4,128)(2,1)}), bf16[16,4,4,512]{3,2,1,0:T(4,128)(2,1)S(1)}, u32[]{:S(2)}, u32[]{:S(2)}) async-start(bf16[16,4,4,512]{3,2,1,0:T(4,128)(2,1)} %broadcast_in_dim.8), calls=%async_computation | async-start | bytes 524288 | tf_op jit(solution)/shard_map/all_to_all | solution.py:176
  20.0 0.7 fusion
  20.7 4.1 %collective-permute-start.1 = (bf16[16,512]{1,0:T(8,128)(2,1)S(1)}, bf16[16,512]{1,0:T(8,128)(2,1)S(1)}, u32[]{:S(2)}, u32[]{:S(2)}) collective-permute-start(bf16[16,512]{1,0:T(8,128)(2,1)S(1)} %get-tuple-element.33), channel_id=1, source_target_pairs={{4,0},{8,4},{12,8},{16,12},{20,16},{24,20},{28,24},{32,28},{36,32}... | collective-permute-start | bytes 49160 | tf_op jit(solution)/shard_map/ppermute | solution.py:198
  24.8 1.9 %collective-permute-start = (bf16[16,512]{1,0:T(8,128)(2,1)S(1)}, bf16[16,512]{1,0:T(8,128)(2,1)S(1)}, u32[]{:S(2)}, u32[]{:S(2)}) collective-permute-start(bf16[16,512]{1,0:T(8,128)(2,1)S(1)} %get-tuple-element.34), channel_id=1, source_target_pairs={{0,4},{4,8},{8,12},{12,16},{16,20},{20,24},{24,28},{28,32},{32,36}... | collective-permute-start | bytes 49160 | tf_op jit(solution)/shard_map/ppermute | solution.py:197
  26.7 11.2 %all-to-all-done = bf16[16,4,4,512]{3,2,1,0:T(4,128)(2,1)S(1)} async-done(((bf16[16,4,4,512]{3,2,1,0:T(4,128)(2,1)}), bf16[16,4,4,512]{3,2,1,0:T(4,128)(2,1)S(1)}, u32[]{:S(2)}, u32[]{:S(2)}) %all-to-all-start) | async-done | bytes 262176 | tf_op jit(solution)/shard_map/all_to_all | solution.py:176
  37.9 0.1 slice.40
  38.0 0.1 copy.8
  38.1 0.1 slice.34
  38.2 0.0 collective-permute-done.1.after
  38.2 0.0 collective-permute-done.prev
  38.2 0.1 broadcast_in_dim.9
  38.3 23.7 %all_to_all.30.in_own = bf16[8,4,16,512]{3,2,1,0:T(8,128)(2,1)} all-to-all(bf16[8,4,16,512]{3,2,1,0:T(8,128)(2,1)S(1)} %broadcast_in_dim.9), channel_id=1, replica_groups={{0,8,16,24,32,40,48,56},{4,12,20,28,36,44,52,60},{64,72,80,88,96,104,11..., dimensions={0} | all-to-all | bytes 1048576 | tf_op jit(solution)/shard_map/all_to_all | solution.py:176
  62.0 0.2 broadcast_in_dim.10
  62.2 0.0 copy-start
  62.2 0.0 copy-start.3
  62.2 0.0 copy-start.4
  62.2 40.8 %all_to_all.31.w_own = bf16[8,3,4,16,512]{4,3,2,1,0:T(8,128)(2,1)S(1)} all-to-all(bf16[8,3,4,16,512]{4,3,2,1,0:T(8,128)(2,1)S(1)} %broadcast_in_dim.10), channel_id=1, replica_groups={{0,8,16,24,32,40,48,56},{4,12,20,28,36,44,52,60},{64,72,80,88,96,104,11..., dimensions={0} | all-to-all | bytes 3145728 | tf_op jit(solution)/shard_map/all_to_all | solution.py:176
  103.0 1.9 %collective-permute-start.6 = (bf16[8,3,4,16,512]{4,3,2,1,0:T(8,128)(2,1)S(1)}, bf16[8,3,4,16,512]{4,3,2,1,0:T(8,128)(2,1)S(1)}, u32[]{:S(2)}, u32[]{:S(2)}) collective-permute-start(bf16[8,3,4,16,512]{4,3,2,1,0:T(8,128)(2,1)S(1)} %all_to_all.31.w_own), channel_id=1, source_target_pairs={{0,4},{4,0},{8,12},{12,8},{16,20},{20,16},{24,28},{28,24},{32,36},... | collective-permute-start | bytes 4718600 | tf_op jit(solution)/shard_map/ppermute | solution.py:195
  104.9 2.4 %collective-permute-start.2 = (bf16[8,4,16,512]{3,2,1,0:T(8,128)(2,1)}, bf16[8,4,16,512]{3,2,1,0:T(8,128)(2,1)}, u32[]{:S(2)}, u32[]{:S(2)}) collective-permute-start(bf16[8,4,16,512]{3,2,1,0:T(8,128)(2,1)} %all_to_all.30.in_own), channel_id=1, source_target_pairs={{0,4},{4,0},{8,12},{12,8},{16,20},{20,16},{24,28},{28,24},{32,36},... | collective-permute-start | bytes 1572872 | tf_op jit(solution)/shard_map/ppermute | solution.py:195
  107.3 0.1 pad_add_fusion.info
  107.4 1.8 %collective-permute-done.2.in_other = bf16[8,4,16,512]{3,2,1,0:T(8,128)(2,1)} collective-permute-done((bf16[8,4,16,512]{3,2,1,0:T(8,128)(2,1)}, bf16[8,4,16,512]{3,2,1,0:T(8,128)(2,1)}, u32[]{:S(2)}, u32[]{:S(2)}) %collective-permute-start.2) | collective-permute-done | bytes 524320 | tf_op jit(solution)/shard_map/ppermute | solution.py:195
  109.2 0.0 copy-done
  109.2 0.0 copy-done.3
  109.2 2.0 %shard_map.73 = (bf16[304,256]{1,0:T(8,128)(2,1)S(1)}, bf16[304,256]{1,0:T(8,128)(2,1)S(1)}, bf16[304,256]{1,0:T(8,128)(2,1)S(1)}, bf16[304,256]{1,0:T(8,128)(2,1)S(1)}) custom-call(s32[3]{0:T(128)S(1)} %pad_add_fusion.info, bf16[16,512]{1,0:T(8,128)(2,1)S(1)} %collective-permute-done.prev, bf16[256,512]{1,0:T(8,128)(2,1)S(1)} %copy-done, ...), custom_call_target="tpu_custom_call" | custom-call | tf_op jit(solution)/shard_map/pallas_call | solution.py:171
  111.2 4.9 %collective-permute-start.3 = (bf16[304,256]{1,0:T(8,128)(2,1)S(1)}, bf16[304,256]{1,0:T(8,128)(2,1)S(1)}, u32[]{:S(2)}, u32[]{:S(2)}) collective-permute-start(bf16[304,256]{1,0:T(8,128)(2,1)S(1)} %get-tuple-element.25), channel_id=1, source_target_pairs={{0,2},{1,3},{2,0},{3,1},{4,6},{5,7},{6,4},{7,5},{8,10},{9,11},{10,... | collective-permute-start | bytes 466952 | tf_op jit(solution)/shard_map/ppermute | solution.py:224
  116.1 2.5 %collective-permute-start.4 = (bf16[304,256]{1,0:T(8,128)(2,1)S(1)}, bf16[304,256]{1,0:T(8,128)(2,1)S(1)}, u32[]{:S(2)}, u32[]{:S(2)}) collective-permute-start(bf16[304,256]{1,0:T(8,128)(2,1)S(1)} %get-tuple-element.26), channel_id=1, source_target_pairs={{0,1},{1,2},{2,3},{3,0},{4,5},{5,6},{6,7},{7,4},{8,9},{9,10},{10,1... | collective-permute-start | bytes 466952 | tf_op jit(solution)/shard_map/ppermute | solution.py:224
  118.6 4.6 %collective-permute-start.5 = (bf16[304,256]{1,0:T(8,128)(2,1)S(1)}, bf16[304,256]{1,0:T(8,128)(2,1)S(1)}, u32[]{:S(2)}, u32[]{:S(2)}) collective-permute-start(bf16[304,256]{1,0:T(8,128)(2,1)S(1)} %get-tuple-element.27), channel_id=1, source_target_pairs={{0,3},{1,0},{2,1},{3,2},{4,7},{5,4},{6,5},{7,6},{8,11},{9,8},{10,9... | collective-permute-start | bytes 466952 | tf_op jit(solution)/shard_map/ppermute | solution.py:224
  123.2 0.0 collective-permute-done.3.refs_1_
  123.2 2.0 %collective-permute-done.4.refs_2_ = bf16[304,256]{1,0:T(8,128)(2,1)S(1)} collective-permute-done((bf16[304,256]{1,0:T(8,128)(2,1)S(1)}, bf16[304,256]{1,0:T(8,128)(2,1)S(1)}, u32[]{:S(2)}, u32[]{:S(2)}) %collective-permute-start.4) | collective-permute-done | bytes 155680 | tf_op jit(solution)/shard_map/ppermute | solution.py:224
  125.2 1.2 collective-permute-done.5.refs_3_
  126.4 0.0 copy-done.4
  126.4 0.0 copy-start.1
  126.4 0.9 copy-done.1
  127.4 1.3 shard_map.74
  128.7 13.3 %all-gather = bf16[1088,256]{1,0:T(8,128)(2,1)S(1)} all-gather(bf16[272,256]{1,0:T(8,128)(2,1)S(1)} %shard_map.74), channel_id=2, replica_groups=mesh['sp'=256,'tp'=4] {'tp'}, dimensions={0}, use_global_device_ids=true | all-gather | bytes 696320 | tf_op jit(solution)/shard_map/all_gather | solution.py:230
  142.0 0.0 collective-permute-done.6.w_other
  142.0 1.2 shard_map.75
  143.3 12.7 %all_to_all.32.refs_0_ = bf16[4,288,256]{2,1,0:T(8,128)(2,1)S(1)} all-to-all(bf16[4,288,256]{2,1,0:T(8,128)(2,1)S(1)} %get-tuple-element.30), channel_id=1, replica_groups=mesh['sp'=256,'tp'=4] {'tp'}, dimensions={0} | all-to-all | bytes 1179648 | tf_op jit(solution)/shard_map/all_to_all | solution.py:215
  156.0 0.0 copy-done.2
  156.0 1.3 shard_map.76
  157.3 10.5 %all_to_all.33.mixed = bf16[4,256,256]{2,1,0:T(8,128)(2,1)S(1)} all-to-all(bf16[4,256,256]{2,1,0:T(8,128)(2,1)S(1)} %shard_map.76), channel_id=1, replica_groups=mesh['sp'=256,'tp'=4] {'tp'}, dimensions={0} | all-to-all | bytes 1048576 | tf_op jit(solution)/shard_map/all_to_all | solution.py:215
  167.8 0.0 copy-start.5
  167.8 0.7 shard_map.77
  168.5 7.8 %all_to_all.34.squares = f32[4,8,256]{2,1,0:T(8,128)S(1)} all-to-all(f32[4,8,256]{2,1,0:T(8,128)S(1)} %get-tuple-element.32), channel_id=1, replica_groups=mesh['sp'=256,'tp'=4] {'tp'}, dimensions={0} | all-to-all | bytes 65536 | tf_op jit(solution)/shard_map/all_to_all | solution.py:215
  176.4 0.0 copy-done.5
  176.4 0.9 shard_map.78
  (4 shorter events, 0.1 us)
Async XLA Ops:
  1.6 36.3 %all-to-all-start = ((bf16[16,4,4,512]{3,2,1,0:T(4,128)(2,1)}), bf16[16,4,4,512]{3,2,1,0:T(4,128)(2,1)S(1)}, u32[]{:S(2)}, u32[]{:S(2)}) async-start(bf16[16,4,4,512]{3,2,1,0:T(4,128)(2,1)} %broadcast_in_dim.8), calls=%async_computation | async-start | bytes 524288 | tf_op jit(solution)/shard_map/all_to_all | solution.py:176
  20.7 17.4 %collective-permute-start.1 = (bf16[16,512]{1,0:T(8,128)(2,1)S(1)}, bf16[16,512]{1,0:T(8,128)(2,1)S(1)}, u32[]{:S(2)}, u32[]{:S(2)}) collective-permute-start(bf16[16,512]{1,0:T(8,128)(2,1)S(1)} %get-tuple-element.33), channel_id=1, source_target_pairs={{4,0},{8,4},{12,8},{16,12},{20,16},{24,20},{28,24},{32,28},{36,32}... | collective-permute-start | bytes 49160 | tf_op jit(solution)/shard_map/ppermute | solution.py:198
  24.8 13.4 %collective-permute-start = (bf16[16,512]{1,0:T(8,128)(2,1)S(1)}, bf16[16,512]{1,0:T(8,128)(2,1)S(1)}, u32[]{:S(2)}, u32[]{:S(2)}) collective-permute-start(bf16[16,512]{1,0:T(8,128)(2,1)S(1)} %get-tuple-element.34), channel_id=1, source_target_pairs={{0,4},{4,8},{8,12},{12,16},{16,20},{20,24},{24,28},{28,32},{32,36}... | collective-permute-start | bytes 49160 | tf_op jit(solution)/shard_map/ppermute | solution.py:197
  62.2 47.0 %copy-start = (bf16[256,512]{1,0:T(8,128)(2,1)S(1)}, bf16[256,512]{1,0:T(8,128)(2,1)}, u32[]{:S(2)}) copy-start(bf16[256,512]{1,0:T(8,128)(2,1)} %own.3) | copy-start | bytes 786436
  62.2 47.0 %copy-start.3 = (f32[2,512]{1,0:T(2,128)S(1)}, f32[2,512]{1,0:T(2,128)}, u32[]{:S(2)}) copy-start(f32[2,512]{1,0:T(2,128)} %gain.3) | copy-start | bytes 12292
  62.2 64.2 %copy-start.4 = (f32[2,256]{1,0:T(2,128)S(1)}, f32[2,256]{1,0:T(2,128)}, u32[]{:S(2)}) copy-start(f32[2,256]{1,0:T(2,128)} %scale.3) | copy-start | bytes 6148
  103.0 39.1 %collective-permute-start.6 = (bf16[8,3,4,16,512]{4,3,2,1,0:T(8,128)(2,1)S(1)}, bf16[8,3,4,16,512]{4,3,2,1,0:T(8,128)(2,1)S(1)}, u32[]{:S(2)}, u32[]{:S(2)}) collective-permute-start(bf16[8,3,4,16,512]{4,3,2,1,0:T(8,128)(2,1)S(1)} %all_to_all.31.w_own), channel_id=1, source_target_pairs={{0,4},{4,0},{8,12},{12,8},{16,20},{20,16},{24,28},{28,24},{32,36},... | collective-permute-start | bytes 4718600 | tf_op jit(solution)/shard_map/ppermute | solution.py:195
  104.9 4.3 %collective-permute-start.2 = (bf16[8,4,16,512]{3,2,1,0:T(8,128)(2,1)}, bf16[8,4,16,512]{3,2,1,0:T(8,128)(2,1)}, u32[]{:S(2)}, u32[]{:S(2)}) collective-permute-start(bf16[8,4,16,512]{3,2,1,0:T(8,128)(2,1)} %all_to_all.30.in_own), channel_id=1, source_target_pairs={{0,4},{4,0},{8,12},{12,8},{16,20},{20,16},{24,28},{28,24},{32,36},... | collective-permute-start | bytes 1572872 | tf_op jit(solution)/shard_map/ppermute | solution.py:195
  111.2 12.0 %collective-permute-start.3 = (bf16[304,256]{1,0:T(8,128)(2,1)S(1)}, bf16[304,256]{1,0:T(8,128)(2,1)S(1)}, u32[]{:S(2)}, u32[]{:S(2)}) collective-permute-start(bf16[304,256]{1,0:T(8,128)(2,1)S(1)} %get-tuple-element.25), channel_id=1, source_target_pairs={{0,2},{1,3},{2,0},{3,1},{4,6},{5,7},{6,4},{7,5},{8,10},{9,11},{10,... | collective-permute-start | bytes 466952 | tf_op jit(solution)/shard_map/ppermute | solution.py:224
  116.1 9.1 %collective-permute-start.4 = (bf16[304,256]{1,0:T(8,128)(2,1)S(1)}, bf16[304,256]{1,0:T(8,128)(2,1)S(1)}, u32[]{:S(2)}, u32[]{:S(2)}) collective-permute-start(bf16[304,256]{1,0:T(8,128)(2,1)S(1)} %get-tuple-element.26), channel_id=1, source_target_pairs={{0,1},{1,2},{2,3},{3,0},{4,5},{5,6},{6,7},{7,4},{8,9},{9,10},{10,1... | collective-permute-start | bytes 466952 | tf_op jit(solution)/shard_map/ppermute | solution.py:224
  118.6 7.8 %collective-permute-start.5 = (bf16[304,256]{1,0:T(8,128)(2,1)S(1)}, bf16[304,256]{1,0:T(8,128)(2,1)S(1)}, u32[]{:S(2)}, u32[]{:S(2)}) collective-permute-start(bf16[304,256]{1,0:T(8,128)(2,1)S(1)} %get-tuple-element.27), channel_id=1, source_target_pairs={{0,3},{1,0},{2,1},{3,2},{4,7},{5,4},{6,5},{7,6},{8,11},{9,8},{10,9... | collective-permute-start | bytes 466952 | tf_op jit(solution)/shard_map/ppermute | solution.py:224
  126.4 1.0 copy-start.1
  142.0 14.0 %copy-start.2 = (bf16[2,1,256,256]{3,2,1,0:T(8,128)(2,1)S(1)}, bf16[2,1,256,256]{3,2,1,0:T(8,128)(2,1)}, u32[]{:S(2)}) copy-start(bf16[2,1,256,256]{3,2,1,0:T(8,128)(2,1)} %wp.3) | copy-start | bytes 786436
  167.8 8.6 %copy-start.5 = (f32[512]{0:T(512)S(1)}, f32[512]{0:T(512)}, u32[]{:S(2)}) copy-start(f32[512]{0:T(512)} %param.13) | copy-start | bytes 6148

commit v2 on v1

--- a/solution.py
+++ b/solution.py
@@ -49,8 +49,8 @@
 
 def group_rows(picks, g):
     parts = []
-    for ref, q in picks:
-        block = ref[:, g] if q is None else ref[:, q, g]
+    for ref, base in picks:
+        block = ref[:, base + g]
         n, rows, d = block.shape
         parts.append(block.reshape(n * rows, d))
     return jnp.concatenate(parts, axis=0)
@@ -73,9 +73,42 @@
         out[rows:] = extra
 
 
+def pack_kernel(w_in, w_out, out):
+    parts = (w_in[0], w_out[0], w_in[1], w_out[1])
+    rows = jnp.concatenate([p.astype(F32) for p in parts], axis=0).astype(BF)
+    for k in range(out.shape[0]):
+        out[k] = rows
+
+
+def sorted_rows(pieces):
+    nz, rows, d = pieces.shape
+    n = nz * rows
+    new = lax.broadcasted_iota(jnp.int32, (n, n), 0)
+    old = lax.broadcasted_iota(jnp.int32, (n, n), 1)
+    weight, z, r = new // (4 * nz), (new >> 2) & (nz - 1), new & 3
+    order = jnp.where(old == z * rows + weight * 4 + r, 1.0, 0.0).astype(BF)
+    done = dot_nn(order, pieces[...].reshape(n, d)).astype(BF)
+    return done.reshape(4, 4, nz, d)
+
+
+def early_kernel(pieces, out):
+    done = sorted_rows(pieces)[0]
+    for k in range(out.shape[0]):
+        out[k] = done
+
+
+def late_kernel(info, pieces, out):
+    done = sorted_rows(pieces)
+    half = jnp.where((info[3] & 1) == 0, done[3, :2].astype(F32), done[3, 2:].astype(F32)).astype(BF)
+    for k in range(out.shape[0]):
+        out[k, :4] = done[1]
+        out[k, 4:8] = done[2]
+        out[k, 8:] = half
+
+
 def first_kernel(info, prev, own, after, gain, in_own, in_other, *outs):
     xf = jnp.concatenate([prev[...].astype(F32), own[...].astype(F32), after[...].astype(F32)], axis=0)
-    project(xf, gain[0:1], ((in_own, None), (in_other, None)), outs, info[0])
+    project(xf, gain[0:1], ((in_own, 0), (in_other, 0)), outs, info[0])
 
 
 def pool_kernel(seq_len, width, halo, layer, copies, info, wp, scale, *refs):
@@ -123,27 +156,30 @@
             out[k] = mixed
 
 
-def added(xf, mixed, picks):
-    total = xf
-    for g in range(mixed.shape[0]):
-        total = total + dot_nn(mixed[g], group_rows(picks, g))
-    return total.astype(BF)
-
-
-def middle_kernel(out_q, in_q, prev, own, after, mixed, gain, w_own, w_other, x_out, pay):
+def middle_kernel(info, prev, own, after, m_0, m_1, m_2, m_3, gain, w_own, w_other, x_out, pay, half):
     xf = jnp.concatenate(
         [prev[...].astype(F32)[8:], own[...].astype(F32), after[...].astype(F32)[:8]], axis=0
     )
-    x = added(xf, mixed, ((w_own, out_q), (w_other, out_q)))
+    total = xf
+    for d, ref in enumerate((m_0, m_1, m_2, m_3)):
+        g = (info[0] - d) & 3
+        total = total + dot_nn(ref[...], group_rows(((w_own, 0), (w_other, 0)), g))
+    x = total.astype(BF)
     x_out[...] = x
+    half[0] = w_own[:, 8:]
+    half[1] = w_other[:, 8:]
     outs = [pay.at[k] for k in range(pay.shape[0])]
-    project(x.astype(F32), gain[1:2], ((w_own, in_q), (w_other, in_q)), outs, 0)
-
-
-def last_kernel(out_q, x_in, mixed, w_own, w_other, x_out, squares):
+    project(x.astype(F32), gain[1:2], ((w_own, 4), (w_other, 4)), outs, 0)
+
+
+def last_kernel(info, x_in, mixed, half, other_half, x_out, squares):
     rows = mixed.shape[1]
-    xf = x_in[...].astype(F32)[MARGIN : MARGIN + rows]
-    x = added(xf, mixed, ((w_own, out_q), (w_other, out_q)))
+    total = x_in[...].astype(F32)[MARGIN : MARGIN + rows]
+    mine = (info[3] & 1) * 2
+    for ref, first in ((half, mine), (other_half, 2 - mine)):
+        for j in range(2):
+            total = total + dot_nn(mixed[first + j], group_rows(((ref.at[0], 0), (ref.at[1], 0)), j))
+    x = total.astype(BF)
     x_out[...] = x
     sums = square_rows(x.astype(F32))[:8]
     for k in range(squares.shape[0]):
@@ -160,22 +196,16 @@
     out[...] = (x_in[...].astype(F32) * r * gain[...]).astype(BF)
 
 
-def call(kernel, shapes, *args, smem=0):
+def call(kernel, shapes, *args, smem=0, near=True):
     spaces = [pltpu.SMEM if i < smem else pltpu.VMEM for i in range(len(args))]
     specs = [pl.BlockSpec(memory_space=space) for space in spaces]
     held = [
-        a if space is pltpu.SMEM else pltpu.with_memory_space_constraint(a, space)
+        a if space is pltpu.SMEM
+        else pltpu.with_memory_space_constraint(a, space if near else pltpu.HBM)
         for a, space in zip(args, spaces)
     ]
     params = pltpu.CompilerParams(vmem_limit_bytes=LIMIT)
     return pl.pallas_call(kernel, out_shape=shapes, in_specs=specs, compiler_params=params)(*held)
-
-
-def to_all(value, axis, groups=None, count=None):
-    count = lax.axis_size(axis) if count is None else count
-    return lax.all_to_all(
-        jnp.broadcast_to(value[None], (count, *value.shape)), axis, 0, 0, axis_index_groups=groups
-    )
 
 
 def shards(resid, norm_gain, w_in, w_pool, pool_scale, w_out, final_gain):
@@ -198,19 +228,26 @@
     after = lax.ppermute(resid[: 2 * MARGIN], "sp", [(i + 1, i) for i in range(n_sp - 1)])
 
     turned = jnp.swapaxes(w_in, 1, 2)
-    mine = jnp.stack([turned[0], w_out[0], turned[1], w_out[1]])
-    along_z = to_all(mine, "sp", z_rings, nz)
-    along_z = jnp.swapaxes(along_z, 0, 1).reshape(4, n_tp, nz // n_tp * 4, block)
-    early, late, before, after = lax.optimization_barrier(
-        (along_z[0], along_z[1:], before, after)
-    )
-    in_own = to_all(early, "sp", y_rings, Y)
+    packed = call(
+        pack_kernel,
+        jax.ShapeDtypeStruct((nz, 16, block), BF),
+        turned, w_out, near=False,
+    )
+    along_z = lax.all_to_all(packed, "sp", 0, 0, axis_index_groups=z_rings)
+    along_z, before, after = lax.optimization_barrier((along_z, before, after))
+    info = jnp.stack([tp, sp & (C - 1), sp * tok, sp >> 4]).astype(jnp.int32)
+    early = call(early_kernel, jax.ShapeDtypeStruct((Y, n_tp, 16, block), BF), along_z)
+    late = call(
+        late_kernel,
+        jax.ShapeDtypeStruct((Y, 10, 16, block), BF),
+        info, along_z, smem=1,
+    )
+    in_own = lax.all_to_all(early, "sp", 0, 0, axis_index_groups=y_rings)
     in_other = send_across(in_own)
     late, in_own = lax.optimization_barrier((late, in_own))
-    own = to_all(late, "sp", y_rings, Y)
+    own = lax.all_to_all(late, "sp", 0, 0, axis_index_groups=y_rings)
     other = send_across(own)
 
-    info = jnp.stack([tp, sp & (C - 1), sp * tok]).astype(jnp.int32)
     wide, mid = tok + 4 * MARGIN, tok + 2 * MARGIN
     exchange = lambda v: lax.all_to_all(v, "tp", 0, 0, tiled=True)
 
@@ -227,15 +264,20 @@
         jax.ShapeDtypeStruct((mid, size), BF),
         info, w_pool, pool_scale, *recv, smem=1,
     )
-    mixed = lax.all_gather(mixed, "tp")
-    x, pay = call(
-        functools.partial(middle_kernel, 0, 1),
+    parts = {0: mixed}
+    for d in (2, 1, 3):
+        parts[d] = lax.ppermute(mixed, "tp", [(i, (i + d) % n_tp) for i in range(n_tp)])
+    x, pay, half = call(
+        middle_kernel,
         (
             jax.ShapeDtypeStruct((mid, block), BF),
             jax.ShapeDtypeStruct((n_tp, mid + ROWS, size), BF),
+            jax.ShapeDtypeStruct((2, Y, 2, 16, block), BF),
         ),
-        before, resid, after, mixed, norm_gain, own, other,
-    )
+        info, before, resid, after, *(parts[d] for d in range(4)), norm_gain, own, other,
+        smem=1,
+    )
+    other_half = lax.ppermute(half, "sp", [(at(z, y, c), at(z ^ 1, y, c)) for z, y, c in places])
     recv = exchange(pay)
     mixed = call(
         functools.partial(pool_kernel, seq_len, width, MARGIN, 1, n_tp),
@@ -244,9 +286,9 @@
     )
     mixed = exchange(mixed)
     x, squares = call(
-        functools.partial(last_kernel, 2),
+        last_kernel,
         (jax.ShapeDtypeStruct((tok, block), BF), jax.ShapeDtypeStruct((n_tp, 8, tok), F32)),
-        x, mixed, own, other,
+        info, x, mixed, half, other_half, smem=1,
     )
     squares = exchange(squares)
     return call(
@@ -267,6 +309,4 @@
         P("tp"),
     )
 
-    return jax.shard_map(
-        shards, mesh=mesh, in_specs=placed, out_specs=P("sp", "tp"), check_vma=False
-    )
+    return jax.shard_map(shards, mesh=mesh, in_specs=placed, out_specs=P("sp", "tp"), check_vma=False)

time: 178 us -> 178 us (level)
  blocking collectives: 109 us -> 43.1 us
  waiting for transfers between devices: 16.2 us -> 52.5 us
  starting transfers between devices: 40.7 us -> 67.2 us
  Pallas kernels: 7.43 us -> 12.8 us
  local copies, waits for them, and re-layouts: 3.74 us -> 0.76 us
    all_to_all x2 -> x1, blocking collectives: 64.5 us -> 35.2 us  [shards(): own = lax.all_to_all(late, 'sp', 0, 0, axis_index_groups=y_rings)]
    all_to_all x1 -> x4, waiting for transfers between devices: 11.2 us -> 36.3 us  [the longest x1 15.8 us: shards(): in_own = lax.all_to_all(early, 'sp', 0, 0, axis_index_groups=y_rings)]
    all_to_all x3 -> x1, blocking collectives: 31 us -> 7.83 us  [shards(): exchange = lambda v: lax.all_to_all(v, 'tp', 0, 0, tiled=True)]
    all_to_all x1 -> x4, starting transfers between devices: 18.4 us -> 32.6 us  [the longest x1 18.4 us: shards(): along_z = lax.all_to_all(packed, 'sp', 0, 0, axis_index_groups=z_rings)]
    all_gather x1 -> x0, blocking collectives: 13.3 us -> none  [shards(): mixed = lax.all_gather(mixed, 'tp')]
    ppermute x0 -> x4, starting transfers between devices: none -> 12.2 us  [the longest x3 10.3 us: shards(): lax.ppermute(mixed, 'tp', [(i, (i + d) % n_tp) for i in range(n_tp)])]
    ppermute x0 -> x4, waiting for transfers between devices: none -> 6.08 us  [the longest x3 6.08 us: shards(): lax.ppermute(mixed, 'tp', [(i, (i + d) % n_tp) for i in range(n_tp)])]
    pallas_call x6 -> x9, Pallas kernels: 7.43 us -> 12.8 us  [call(): pl.pallas_call(kernel, out_shape=shapes, in_specs=specs, compiler_params=...]
  transfers between devices with their start and end apart: 8 -> 15, of which waited for: 4 -> 12; matrix products, arithmetic and copies ran while one was open for 1% -> 0% of each run, Pallas kernels for 2% -> 3%
where the time goes in v2:
time: 178 us; the launch traced here: 177 us
  starting transfers between devices  67.2 us (38%)
  waiting for transfers between devices  52.5 us (29%)
  blocking collectives  43.1 us (24%)
  Pallas kernels  12.8 us (7%)
    all_to_all x1, blocking collectives, shards(): own = lax.all_to_all(late, 'sp', 0, 0, axis_index_groups=y_rings)  35.2 us
    all_to_all x1, starting transfers between devices, shards(): along_z = lax.all_to_all(packed, 'sp', 0, 0, axis_index_groups=z_rings)  18.4 us
    all_to_all x1, waiting for transfers between devices, shards(): in_own = lax.all_to_all(early, 'sp', 0, 0, axis_index_groups=y_rings)  15.8 us
    all_to_all x2, waiting for transfers between devices, shards(): exchange = lambda v: lax.all_to_all(v, 'tp', 0, 0, tiled=True)  14.7 us
    pallas_call x9, Pallas kernels, call(): pl.pallas_call(kernel, out_shape=shapes, in_specs=specs, compiler_params=...  12.8 us
    ppermute x3, starting transfers between devices, shards(): lax.ppermute(pay[d], 'tp', [(i, (i + d) % n_tp) for i in range(n_tp)])  12 us
    ppermute x3, starting transfers between devices, shards(): lax.ppermute(mixed, 'tp', [(i, (i + d) % n_tp) for i in range(n_tp)])  10.3 us
    all_to_all x1, blocking collectives, shards(): exchange = lambda v: lax.all_to_all(v, 'tp', 0, 0, tiled=True)  7.83 us
  transfers between devices with their start and end apart: 15, of which 12 were waited for; matrix products, arithmetic and copies ran while one was open for 0% of the time, Pallas kernels for 3%

profile of v2, /device:TPU:64, one launch (start us, length us, event | category | flops | bytes accessed | tf_op | source)
XLA Modules:
  0.0 176.5 jit_solution(13249260804026097470)
XLA Ops:
  0.0 1.4 shard_map.73
  1.4 18.4 %all-to-all-start = ((bf16[16,16,512]{2,1,0:T(8,128)(2,1)}), bf16[16,16,512]{2,1,0:T(8,128)(2,1)S(1)}, u32[]{:S(2)}, u32[]{:S(2)}) async-start(bf16[16,16,512]{2,1,0:T(8,128)(2,1)} %shard_map.73), calls=%async_computation | async-start | bytes 524288 | tf_op jit(solution)/shard_map/all_to_all | solution.py:236
  19.9 0.7 fusion
  20.6 4.1 %collective-permute-start.1 = (bf16[16,512]{1,0:T(8,128)(2,1)S(1)}, bf16[16,512]{1,0:T(8,128)(2,1)S(1)}, u32[]{:S(2)}, u32[]{:S(2)}) collective-permute-start(bf16[16,512]{1,0:T(8,128)(2,1)S(1)} %get-tuple-element.33), channel_id=1, source_target_pairs={{4,0},{8,4},{12,8},{16,12},{20,16},{24,20},{28,24},{32,28},{36,32}... | collective-permute-start | bytes 49160 | tf_op jit(solution)/shard_map/ppermute | solution.py:228
  24.7 1.9 %collective-permute-start = (bf16[16,512]{1,0:T(8,128)(2,1)S(1)}, bf16[16,512]{1,0:T(8,128)(2,1)S(1)}, u32[]{:S(2)}, u32[]{:S(2)}) collective-permute-start(bf16[16,512]{1,0:T(8,128)(2,1)S(1)} %get-tuple-element.34), channel_id=1, source_target_pairs={{0,4},{4,8},{8,12},{12,16},{16,20},{20,24},{24,28},{28,32},{32,36}... | collective-permute-start | bytes 49160 | tf_op jit(solution)/shard_map/ppermute | solution.py:227
  26.6 3.4 %collective-permute-done.1.after = bf16[16,512]{1,0:T(8,128)(2,1)S(1)} collective-permute-done((bf16[16,512]{1,0:T(8,128)(2,1)S(1)}, bf16[16,512]{1,0:T(8,128)(2,1)S(1)}, u32[]{:S(2)}, u32[]{:S(2)}) %collective-permute-start.1) | collective-permute-done | bytes 16416 | tf_op jit(solution)/shard_map/ppermute | solution.py:228
  30.0 1.9 %collective-permute-done.prev = bf16[16,512]{1,0:T(8,128)(2,1)S(1)} collective-permute-done((bf16[16,512]{1,0:T(8,128)(2,1)S(1)}, bf16[16,512]{1,0:T(8,128)(2,1)S(1)}, u32[]{:S(2)}, u32[]{:S(2)}) %collective-permute-start) | collective-permute-done | bytes 16416 | tf_op jit(solution)/shard_map/ppermute | solution.py:227
  31.9 5.9 %all-to-all-done.pieces = bf16[16,16,512]{2,1,0:T(8,128)(2,1)S(1)} async-done(((bf16[16,16,512]{2,1,0:T(8,128)(2,1)}), bf16[16,16,512]{2,1,0:T(8,128)(2,1)S(1)}, u32[]{:S(2)}, u32[]{:S(2)}) %all-to-all-start) | async-done | bytes 262176 | tf_op jit(solution)/shard_map/all_to_all | solution.py:236
  37.8 1.0 shard_map.75
  38.8 7.1 %all-to-all-start.1 = ((bf16[8,4,16,512]{3,2,1,0:T(8,128)(2,1)}), bf16[8,4,16,512]{3,2,1,0:T(8,128)(2,1)S(1)}, u32[]{:S(2)}, u32[]{:S(2)}) async-start(bf16[8,4,16,512]{3,2,1,0:T(8,128)(2,1)} %shard_map.75), calls=%async_computation.1 | async-start | bytes 1048576 | tf_op jit(solution)/shard_map/all_to_all | solution.py:245
  45.9 0.1 pad_add_fusion.info
  46.0 0.8 shard_map.74
  46.8 0.0 copy-start
  46.8 0.0 copy-start.2
  46.8 15.8 %all-to-all-done.1.in_own = bf16[8,4,16,512]{3,2,1,0:T(8,128)(2,1)S(1)} async-done(((bf16[8,4,16,512]{3,2,1,0:T(8,128)(2,1)}), bf16[8,4,16,512]{3,2,1,0:T(8,128)(2,1)S(1)}, u32[]{:S(2)}, u32[]{:S(2)}) %all-to-all-start.1) | async-done | bytes 524320 | tf_op jit(solution)/shard_map/all_to_all | solution.py:245
  62.6 35.2 %all_to_all.30.w_own = bf16[8,10,16,512]{3,2,1,0:T(8,128)(2,1)S(1)} all-to-all(bf16[8,10,16,512]{3,2,1,0:T(8,128)(2,1)S(1)} %shard_map.74), channel_id=1, replica_groups={{0,8,16,24,32,40,48,56},{4,12,20,28,36,44,52,60},{64,72,80,88,96,104,11..., dimensions={0} | all-to-all | bytes 2621440 | tf_op jit(solution)/shard_map/all_to_all | solution.py:248
  97.8 2.0 %collective-permute-start.9 = (bf16[8,10,16,512]{3,2,1,0:T(8,128)(2,1)S(1)}, bf16[8,10,16,512]{3,2,1,0:T(8,128)(2,1)S(1)}, u32[]{:S(2)}, u32[]{:S(2)}) collective-permute-start(bf16[8,10,16,512]{3,2,1,0:T(8,128)(2,1)S(1)} %all_to_all.30.w_own), channel_id=1, source_target_pairs={{0,4},{4,0},{8,12},{12,8},{16,20},{20,16},{24,28},{28,24},{32,36},... | collective-permute-start | bytes 3932168 | tf_op jit(solution)/shard_map/ppermute | solution.py:225
  99.9 2.4 %collective-permute-start.2 = (bf16[8,4,16,512]{3,2,1,0:T(8,128)(2,1)S(1)}, bf16[8,4,16,512]{3,2,1,0:T(8,128)(2,1)S(1)}, u32[]{:S(2)}, u32[]{:S(2)}) collective-permute-start(bf16[8,4,16,512]{3,2,1,0:T(8,128)(2,1)S(1)} %all-to-all-done.1.in_own), channel_id=1, source_target_pairs={{0,4},{4,0},{8,12},{12,8},{16,20},{20,16},{24,28},{28,24},{32,36},... | collective-permute-start | bytes 1572872 | tf_op jit(solution)/shard_map/ppermute | solution.py:225
  102.3 1.5 collective-permute-done.2.in_other
  103.8 0.0 copy-done
  103.8 1.3 shard_map.76
  105.2 4.9 %collective-permute-start.3 = (bf16[304,256]{1,0:T(8,128)(2,1)S(1)}, bf16[304,256]{1,0:T(8,128)(2,1)S(1)}, u32[]{:S(2)}, u32[]{:S(2)}) collective-permute-start(bf16[304,256]{1,0:T(8,128)(2,1)S(1)} %get-tuple-element.24), channel_id=1, source_target_pairs={{0,2},{1,3},{2,0},{3,1},{4,6},{5,7},{6,4},{7,5},{8,10},{9,11},{10,... | collective-permute-start | bytes 466952 | tf_op jit(solution)/shard_map/ppermute | solution.py:261
  110.1 2.5 %collective-permute-start.4 = (bf16[304,256]{1,0:T(8,128)(2,1)S(1)}, bf16[304,256]{1,0:T(8,128)(2,1)S(1)}, u32[]{:S(2)}, u32[]{:S(2)}) collective-permute-start(bf16[304,256]{1,0:T(8,128)(2,1)S(1)} %get-tuple-element.25), channel_id=1, source_target_pairs={{0,1},{1,2},{2,3},{3,0},{4,5},{5,6},{6,7},{7,4},{8,9},{9,10},{10,1... | collective-permute-start | bytes 466952 | tf_op jit(solution)/shard_map/ppermute | solution.py:261
  112.6 4.6 %collective-permute-start.5 = (bf16[304,256]{1,0:T(8,128)(2,1)S(1)}, bf16[304,256]{1,0:T(8,128)(2,1)S(1)}, u32[]{:S(2)}, u32[]{:S(2)}) collective-permute-start(bf16[304,256]{1,0:T(8,128)(2,1)S(1)} %get-tuple-element.26), channel_id=1, source_target_pairs={{0,3},{1,0},{2,1},{3,2},{4,7},{5,4},{6,5},{7,6},{8,11},{9,8},{10,9... | collective-permute-start | bytes 466952 | tf_op jit(solution)/shard_map/ppermute | solution.py:261
  117.2 0.0 collective-permute-done.3.refs_1_
  117.2 2.0 %collective-permute-done.4.refs_2_ = bf16[304,256]{1,0:T(8,128)(2,1)S(1)} collective-permute-done((bf16[304,256]{1,0:T(8,128)(2,1)S(1)}, bf16[304,256]{1,0:T(8,128)(2,1)S(1)}, u32[]{:S(2)}, u32[]{:S(2)}) %collective-permute-start.4) | collective-permute-done | bytes 155680 | tf_op jit(solution)/shard_map/ppermute | solution.py:261
  119.2 1.2 collective-permute-done.5.refs_3_
  120.4 0.0 copy-done.3
  120.4 1.3 shard_map.77.m_0
  121.7 5.6 %collective-permute-start.8 = (bf16[272,256]{1,0:T(8,128)(2,1)S(1)}, bf16[272,256]{1,0:T(8,128)(2,1)S(1)}, u32[]{:S(2)}, u32[]{:S(2)}) collective-permute-start(bf16[272,256]{1,0:T(8,128)(2,1)S(1)} %shard_map.77.m_0), channel_id=1, source_target_pairs={{0,3},{1,0},{2,1},{3,2},{4,7},{5,4},{6,5},{7,6},{8,11},{9,8},{10,9... | collective-permute-start | bytes 417800 | tf_op jit(solution)/shard_map/ppermute | solution.py:269
  127.4 1.9 %collective-permute-start.7 = (bf16[272,256]{1,0:T(8,128)(2,1)S(1)}, bf16[272,256]{1,0:T(8,128)(2,1)S(1)}, u32[]{:S(2)}, u32[]{:S(2)}) collective-permute-start(bf16[272,256]{1,0:T(8,128)(2,1)S(1)} %shard_map.77.m_0), channel_id=1, source_target_pairs={{0,2},{1,3},{2,0},{3,1},{4,6},{5,7},{6,4},{7,5},{8,10},{9,11},{10,... | collective-permute-start | bytes 417800 | tf_op jit(solution)/shard_map/ppermute | solution.py:269
  129.3 2.8 %collective-permute-start.6 = (bf16[272,256]{1,0:T(8,128)(2,1)S(1)}, bf16[272,256]{1,0:T(8,128)(2,1)S(1)}, u32[]{:S(2)}, u32[]{:S(2)}) collective-permute-start(bf16[272,256]{1,0:T(8,128)(2,1)S(1)} %shard_map.77.m_0), channel_id=1, source_target_pairs={{0,1},{1,2},{2,3},{3,0},{4,5},{5,6},{6,7},{7,4},{8,9},{9,10},{10,1... | collective-permute-start | bytes 417800 | tf_op jit(solution)/shard_map/ppermute | solution.py:269
  132.1 0.9 collective-permute-done.8.m_3
  132.9 4.1 %collective-permute-done.7.m_2 = bf16[272,256]{1,0:T(8,128)(2,1)S(1)} collective-permute-done((bf16[272,256]{1,0:T(8,128)(2,1)S(1)}, bf16[272,256]{1,0:T(8,128)(2,1)S(1)}, u32[]{:S(2)}, u32[]{:S(2)}) %collective-permute-start.7) | collective-permute-done | bytes 139296 | tf_op jit(solution)/shard_map/ppermute | solution.py:269
  137.0 1.1 collective-permute-done.6.m_1
  138.1 0.0 collective-permute-done.9.w_other
  138.1 2.6 %shard_map.78 = (bf16[272,512]{1,0:T(8,128)(2,1)S(1)}, bf16[4,288,256]{2,1,0:T(8,128)(2,1)}, bf16[2,8,2,16,512]{4,3,2,1,0:T(8,128)(2,1)S(1)}) custom-call(s32[4]{0:T(128)S(1)} %pad_add_fusion.info, bf16[16,512]{1,0:T(8,128)(2,1)S(1)} %collective-permute-done.prev, bf16[256,512]{1,0:T(8,128)(2,1)S(1)} %copy-done, ...), custom_call_target="tpu_custom_call" | custom-call | tf_op jit(solution)/shard_map/pallas_call | solution.py:208
  140.8 3.5 %all-to-all-start.3 = ((bf16[4,288,256]{2,1,0:T(8,128)(2,1)}), bf16[4,288,256]{2,1,0:T(8,128)(2,1)S(1)}, u32[]{:S(2)}, u32[]{:S(2)}) async-start(bf16[4,288,256]{2,1,0:T(8,128)(2,1)} %get-tuple-element.29), calls=%async_computation.3 | async-start | bytes 1179648 | tf_op jit(solution)/shard_map/all_to_all | solution.py:252
  144.3 1.9 %collective-permute-start.10 = (bf16[2,8,2,16,512]{4,3,2,1,0:T(8,128)(2,1)S(1)}, bf16[2,8,2,16,512]{4,3,2,1,0:T(8,128)(2,1)S(1)}, u32[]{:S(2)}, u32[]{:S(2)}) collective-permute-start(bf16[2,8,2,16,512]{4,3,2,1,0:T(8,128)(2,1)S(1)} %get-tuple-element.30.half), channel_id=1, source_target_pairs={{0,64},{4,68},{8,72},{12,76},{16,80},{20,84},{24,88},{28,92},{32,9... | collective-permute-start | bytes 1572872 | tf_op jit(solution)/shard_map/ppermute | solution.py:280
  146.2 6.6 %all-to-all-done.3.refs_0_ = bf16[4,288,256]{2,1,0:T(8,128)(2,1)S(1)} async-done(((bf16[4,288,256]{2,1,0:T(8,128)(2,1)}), bf16[4,288,256]{2,1,0:T(8,128)(2,1)S(1)}, u32[]{:S(2)}, u32[]{:S(2)}) %all-to-all-start.3) | async-done | bytes 589856 | tf_op jit(solution)/shard_map/all_to_all | solution.py:252
  152.8 2.1 %shard_map.79 = bf16[4,256,256]{2,1,0:T(8,128)(2,1)} custom-call(s32[4]{0:T(128)S(1)} %pad_add_fusion.info, bf16[2,1,256,256]{3,2,1,0:T(8,128)(2,1)S(1)} %copy-done.1, f32[2,256]{1,0:T(2,128)S(1)} %copy-done.3, bf16[4,288,256]{2,1,0:T(8,128)(2,1)S(1)} %all-to-all-done.3.refs_0_), custom_call_target="tpu_custom_call" | custom-call | tf_op jit(solution)/shard_map/pallas_call | solution.py:208
  154.9 3.6 %all-to-all-start.4 = ((bf16[4,256,256]{2,1,0:T(8,128)(2,1)}), bf16[4,256,256]{2,1,0:T(8,128)(2,1)S(1)}, u32[]{:S(2)}, u32[]{:S(2)}) async-start(bf16[4,256,256]{2,1,0:T(8,128)(2,1)} %shard_map.79), calls=%async_computation.4 | async-start | bytes 1048576 | tf_op jit(solution)/shard_map/all_to_all | solution.py:252
  158.5 0.0 collective-permute-done.10.other_half
  158.5 8.0 %all-to-all-done.4.mixed = bf16[4,256,256]{2,1,0:T(8,128)(2,1)S(1)} async-done(((bf16[4,256,256]{2,1,0:T(8,128)(2,1)}), bf16[4,256,256]{2,1,0:T(8,128)(2,1)S(1)}, u32[]{:S(2)}, u32[]{:S(2)}) %all-to-all-start.4) | async-done | bytes 524320 | tf_op jit(solution)/shard_map/all_to_all | solution.py:252
  166.6 1.3 shard_map.80
  167.9 7.8 %all_to_all.31.squares = f32[4,8,256]{2,1,0:T(8,128)S(1)} all-to-all(f32[4,8,256]{2,1,0:T(8,128)S(1)} %get-tuple-element.32), channel_id=1, replica_groups=mesh['sp'=256,'tp'=4] {'tp'}, dimensions={0} | all-to-all | bytes 65536 | tf_op jit(solution)/shard_map/all_to_all | solution.py:252
  175.7 0.0 copy-done.4
  175.7 0.9 shard_map.81
  (5 shorter events, 0.0 us)
Async XLA Ops:
  1.4 36.3 %all-to-all-start = ((bf16[16,16,512]{2,1,0:T(8,128)(2,1)}), bf16[16,16,512]{2,1,0:T(8,128)(2,1)S(1)}, u32[]{:S(2)}, u32[]{:S(2)}) async-start(bf16[16,16,512]{2,1,0:T(8,128)(2,1)} %shard_map.73), calls=%async_computation | async-start | bytes 524288 | tf_op jit(solution)/shard_map/all_to_all | solution.py:236
  20.6 9.4 %collective-permute-start.1 = (bf16[16,512]{1,0:T(8,128)(2,1)S(1)}, bf16[16,512]{1,0:T(8,128)(2,1)S(1)}, u32[]{:S(2)}, u32[]{:S(2)}) collective-permute-start(bf16[16,512]{1,0:T(8,128)(2,1)S(1)} %get-tuple-element.33), channel_id=1, source_target_pairs={{4,0},{8,4},{12,8},{16,12},{20,16},{24,20},{28,24},{32,28},{36,32}... | collective-permute-start | bytes 49160 | tf_op jit(solution)/shard_map/ppermute | solution.py:228
  24.7 7.2 %collective-permute-start = (bf16[16,512]{1,0:T(8,128)(2,1)S(1)}, bf16[16,512]{1,0:T(8,128)(2,1)S(1)}, u32[]{:S(2)}, u32[]{:S(2)}) collective-permute-start(bf16[16,512]{1,0:T(8,128)(2,1)S(1)} %get-tuple-element.34), channel_id=1, source_target_pairs={{0,4},{4,8},{8,12},{12,16},{16,20},{20,24},{24,28},{28,32},{32,36}... | collective-permute-start | bytes 49160 | tf_op jit(solution)/shard_map/ppermute | solution.py:227
  38.8 23.8 %all-to-all-start.1 = ((bf16[8,4,16,512]{3,2,1,0:T(8,128)(2,1)}), bf16[8,4,16,512]{3,2,1,0:T(8,128)(2,1)S(1)}, u32[]{:S(2)}, u32[]{:S(2)}) async-start(bf16[8,4,16,512]{3,2,1,0:T(8,128)(2,1)} %shard_map.75), calls=%async_computation.1 | async-start | bytes 1048576 | tf_op jit(solution)/shard_map/all_to_all | solution.py:245
  46.8 57.0 %copy-start = (bf16[256,512]{1,0:T(8,128)(2,1)S(1)}, bf16[256,512]{1,0:T(8,128)(2,1)}, u32[]{:S(2)}) copy-start(bf16[256,512]{1,0:T(8,128)(2,1)} %own.3) | copy-start | bytes 786436
  46.8 57.0 %copy-start.2 = (f32[2,512]{1,0:T(2,128)S(1)}, f32[2,512]{1,0:T(2,128)}, u32[]{:S(2)}) copy-start(f32[2,512]{1,0:T(2,128)} %gain.3) | copy-start | bytes 12292
  97.8 22.6 %copy-start.1 = (bf16[2,1,256,256]{3,2,1,0:T(8,128)(2,1)S(1)}, bf16[2,1,256,256]{3,2,1,0:T(8,128)(2,1)}, u32[]{:S(2)}) copy-start(bf16[2,1,256,256]{3,2,1,0:T(8,128)(2,1)} %wp.3) | copy-start | bytes 786436
  97.8 22.6 %copy-start.3 = (f32[2,256]{1,0:T(2,128)S(1)}, f32[2,256]{1,0:T(2,128)}, u32[]{:S(2)}) copy-start(f32[2,256]{1,0:T(2,128)} %scale.3) | copy-start | bytes 6148
  97.8 40.3 %collective-permute-start.9 = (bf16[8,10,16,512]{3,2,1,0:T(8,128)(2,1)S(1)}, bf16[8,10,16,512]{3,2,1,0:T(8,128)(2,1)S(1)}, u32[]{:S(2)}, u32[]{:S(2)}) collective-permute-start(bf16[8,10,16,512]{3,2,1,0:T(8,128)(2,1)S(1)} %all_to_all.30.w_own), channel_id=1, source_target_pairs={{0,4},{4,0},{8,12},{12,8},{16,20},{20,16},{24,28},{28,24},{32,36},... | collective-permute-start | bytes 3932168 | tf_op jit(solution)/shard_map/ppermute | solution.py:225
  99.9 3.9 %collective-permute-start.2 = (bf16[8,4,16,512]{3,2,1,0:T(8,128)(2,1)S(1)}, bf16[8,4,16,512]{3,2,1,0:T(8,128)(2,1)S(1)}, u32[]{:S(2)}, u32[]{:S(2)}) collective-permute-start(bf16[8,4,16,512]{3,2,1,0:T(8,128)(2,1)S(1)} %all-to-all-done.1.in_own), channel_id=1, source_target_pairs={{0,4},{4,0},{8,12},{12,8},{16,20},{20,16},{24,28},{28,24},{32,36},... | collective-permute-start | bytes 1572872 | tf_op jit(solution)/shard_map/ppermute | solution.py:225
  105.2 12.0 %collective-permute-start.3 = (bf16[304,256]{1,0:T(8,128)(2,1)S(1)}, bf16[304,256]{1,0:T(8,128)(2,1)S(1)}, u32[]{:S(2)}, u32[]{:S(2)}) collective-permute-start(bf16[304,256]{1,0:T(8,128)(2,1)S(1)} %get-tuple-element.24), channel_id=1, source_target_pairs={{0,2},{1,3},{2,0},{3,1},{4,6},{5,7},{6,4},{7,5},{8,10},{9,11},{10,... | collective-permute-start | bytes 466952 | tf_op jit(solution)/shard_map/ppermute | solution.py:261
  110.1 9.1 %collective-permute-start.4 = (bf16[304,256]{1,0:T(8,128)(2,1)S(1)}, bf16[304,256]{1,0:T(8,128)(2,1)S(1)}, u32[]{:S(2)}, u32[]{:S(2)}) collective-permute-start(bf16[304,256]{1,0:T(8,128)(2,1)S(1)} %get-tuple-element.25), channel_id=1, source_target_pairs={{0,1},{1,2},{2,3},{3,0},{4,5},{5,6},{6,7},{7,4},{8,9},{9,10},{10,1... | collective-permute-start | bytes 466952 | tf_op jit(solution)/shard_map/ppermute | solution.py:261
  112.6 7.8 %collective-permute-start.5 = (bf16[304,256]{1,0:T(8,128)(2,1)S(1)}, bf16[304,256]{1,0:T(8,128)(2,1)S(1)}, u32[]{:S(2)}, u32[]{:S(2)}) collective-permute-start(bf16[304,256]{1,0:T(8,128)(2,1)S(1)} %get-tuple-element.26), channel_id=1, source_target_pairs={{0,3},{1,0},{2,1},{3,2},{4,7},{5,4},{6,5},{7,6},{8,11},{9,8},{10,9... | collective-permute-start | bytes 466952 | tf_op jit(solution)/shard_map/ppermute | solution.py:261
  121.7 11.2 %collective-permute-start.8 = (bf16[272,256]{1,0:T(8,128)(2,1)S(1)}, bf16[272,256]{1,0:T(8,128)(2,1)S(1)}, u32[]{:S(2)}, u32[]{:S(2)}) collective-permute-start(bf16[272,256]{1,0:T(8,128)(2,1)S(1)} %shard_map.77.m_0), channel_id=1, source_target_pairs={{0,3},{1,0},{2,1},{3,2},{4,7},{5,4},{6,5},{7,6},{8,11},{9,8},{10,9... | collective-permute-start | bytes 417800 | tf_op jit(solution)/shard_map/ppermute | solution.py:269
  127.4 9.7 %collective-permute-start.7 = (bf16[272,256]{1,0:T(8,128)(2,1)S(1)}, bf16[272,256]{1,0:T(8,128)(2,1)S(1)}, u32[]{:S(2)}, u32[]{:S(2)}) collective-permute-start(bf16[272,256]{1,0:T(8,128)(2,1)S(1)} %shard_map.77.m_0), channel_id=1, source_target_pairs={{0,2},{1,3},{2,0},{3,1},{4,6},{5,7},{6,4},{7,5},{8,10},{9,11},{10,... | collective-permute-start | bytes 417800 | tf_op jit(solution)/shard_map/ppermute | solution.py:269
  129.3 8.9 %collective-permute-start.6 = (bf16[272,256]{1,0:T(8,128)(2,1)S(1)}, bf16[272,256]{1,0:T(8,128)(2,1)S(1)}, u32[]{:S(2)}, u32[]{:S(2)}) collective-permute-start(bf16[272,256]{1,0:T(8,128)(2,1)S(1)} %shard_map.77.m_0), channel_id=1, source_target_pairs={{0,1},{1,2},{2,3},{3,0},{4,5},{5,6},{6,7},{7,4},{8,9},{9,10},{10,1... | collective-permute-start | bytes 417800 | tf_op jit(solution)/shard_map/ppermute | solution.py:269
  140.8 12.1 %all-to-all-start.3 = ((bf16[4,288,256]{2,1,0:T(8,128)(2,1)}), bf16[4,288,256]{2,1,0:T(8,128)(2,1)S(1)}, u32[]{:S(2)}, u32[]{:S(2)}) async-start(bf16[4,288,256]{2,1,0:T(8,128)(2,1)} %get-tuple-element.29), calls=%async_computation.3 | async-start | bytes 1179648 | tf_op jit(solution)/shard_map/all_to_all | solution.py:252
  144.3 14.3 %collective-permute-start.10 = (bf16[2,8,2,16,512]{4,3,2,1,0:T(8,128)(2,1)S(1)}, bf16[2,8,2,16,512]{4,3,2,1,0:T(8,128)(2,1)S(1)}, u32[]{:S(2)}, u32[]{:S(2)}) collective-permute-start(bf16[2,8,2,16,512]{4,3,2,1,0:T(8,128)(2,1)S(1)} %get-tuple-element.30.half), channel_id=1, source_target_pairs={{0,64},{4,68},{8,72},{12,76},{16,80},{20,84},{24,88},{28,92},{32,9... | collective-permute-start | bytes 1572872 | tf_op jit(solution)/shard_map/ppermute | solution.py:280
  154.9 20.8 %copy-start.4 = (f32[512]{0:T(512)S(1)}, f32[512]{0:T(512)}, u32[]{:S(2)}) copy-start(f32[512]{0:T(512)} %param.13) | copy-start | bytes 6148
  154.9 11.7 %all-to-all-start.4 = ((bf16[4,256,256]{2,1,0:T(8,128)(2,1)}), bf16[4,256,256]{2,1,0:T(8,128)(2,1)S(1)}, u32[]{:S(2)}, u32[]{:S(2)}) async-start(bf16[4,256,256]{2,1,0:T(8,128)(2,1)} %shard_map.79), calls=%async_computation.4 | async-start | bytes 1048576 | tf_op jit(solution)/shard_map/all_to_all | solution.py:252

commit v3 on v2

--- a/solution.py
+++ b/solution.py
@@ -80,29 +80,29 @@
         out[k] = rows
 
 
-def sorted_rows(pieces):
+def sorted_rows(pieces, first, count):
     nz, rows, d = pieces.shape
-    n = nz * rows
-    new = lax.broadcasted_iota(jnp.int32, (n, n), 0)
-    old = lax.broadcasted_iota(jnp.int32, (n, n), 1)
-    weight, z, r = new // (4 * nz), (new >> 2) & (nz - 1), new & 3
+    shape = (count * 4 * nz, nz * rows)
+    new = lax.broadcasted_iota(jnp.int32, shape, 0)
+    old = lax.broadcasted_iota(jnp.int32, shape, 1)
+    weight, z, r = first + jnp.right_shift(new, (4 * nz).bit_length() - 1), (new >> 2) & (nz - 1), new & 3
     order = jnp.where(old == z * rows + weight * 4 + r, 1.0, 0.0).astype(BF)
-    done = dot_nn(order, pieces[...].reshape(n, d)).astype(BF)
-    return done.reshape(4, 4, nz, d)
+    done = dot_nn(order, pieces[...].reshape(nz * rows, d)).astype(BF)
+    return done.reshape(count, 4, nz, d)
 
 
 def early_kernel(pieces, out):
-    done = sorted_rows(pieces)[0]
+    done = sorted_rows(pieces, 0, 1)[0]
     for k in range(out.shape[0]):
         out[k] = done
 
 
 def late_kernel(info, pieces, out):
-    done = sorted_rows(pieces)
-    half = jnp.where((info[3] & 1) == 0, done[3, :2].astype(F32), done[3, 2:].astype(F32)).astype(BF)
+    done = sorted_rows(pieces, 1, 3)
+    half = jnp.where((info[3] & 1) == 0, done[2, :2].astype(F32), done[2, 2:].astype(F32)).astype(BF)
     for k in range(out.shape[0]):
-        out[k, :4] = done[1]
-        out[k, 4:8] = done[2]
+        out[k, :4] = done[0]
+        out[k, 4:8] = done[1]
         out[k, 8:] = half
 
 

time: 178 us -> 178 us (level)
  no operation moved by 1% of the time
where the time goes in v3:
time: 178 us; the launch traced here: 177 us
  starting transfers between devices  67.2 us (38%)
  waiting for transfers between devices  52.5 us (29%)
  blocking collectives  43.1 us (24%)
  Pallas kernels  12.8 us (7%)
    all_to_all x1, blocking collectives, shards(): own = lax.all_to_all(late, 'sp', 0, 0, axis_index_groups=y_rings)  35.2 us
    all_to_all x1, starting transfers between devices, shards(): along_z = lax.all_to_all(packed, 'sp', 0, 0, axis_index_groups=z_rings)  18.4 us
    all_to_all x1, waiting for transfers between devices, shards(): in_own = lax.all_to_all(early, 'sp', 0, 0, axis_index_groups=y_rings)  15.8 us
    all_to_all x2, waiting for transfers between devices, shards(): exchange = lambda v: lax.all_to_all(v, 'tp', 0, 0, tiled=True)  14.7 us
    pallas_call x9, Pallas kernels, call(): pl.pallas_call(kernel, out_shape=shapes, in_specs=specs, compiler_params=...  12.8 us
    ppermute x3, starting transfers between devices, shards(): lax.ppermute(pay[d], 'tp', [(i, (i + d) % n_tp) for i in range(n_tp)])  12 us
    ppermute x3, starting transfers between devices, shards(): lax.ppermute(mixed, 'tp', [(i, (i + d) % n_tp) for i in range(n_tp)])  10.3 us
    all_to_all x1, blocking collectives, shards(): exchange = lambda v: lax.all_to_all(v, 'tp', 0, 0, tiled=True)  7.83 us
  transfers between devices with their start and end apart: 15, of which 12 were waited for; matrix products, arithmetic and copies ran while one was open for 0% of the time, Pallas kernels for 3%

profile of v3, /device:TPU:64, one launch (start us, length us, event | category | flops | bytes accessed | tf_op | source)
XLA Modules:
  0.0 176.5 jit_solution(255266718465092595)
XLA Ops:
  0.0 1.4 shard_map.73
  1.4 18.4 %all-to-all-start = ((bf16[16,16,512]{2,1,0:T(8,128)(2,1)}), bf16[16,16,512]{2,1,0:T(8,128)(2,1)S(1)}, u32[]{:S(2)}, u32[]{:S(2)}) async-start(bf16[16,16,512]{2,1,0:T(8,128)(2,1)} %shard_map.73), calls=%async_computation | async-start | bytes 524288 | tf_op jit(solution)/shard_map/all_to_all | solution.py:236
  19.9 0.7 fusion
  20.6 4.1 %collective-permute-start.1 = (bf16[16,512]{1,0:T(8,128)(2,1)S(1)}, bf16[16,512]{1,0:T(8,128)(2,1)S(1)}, u32[]{:S(2)}, u32[]{:S(2)}) collective-permute-start(bf16[16,512]{1,0:T(8,128)(2,1)S(1)} %get-tuple-element.33), channel_id=1, source_target_pairs={{4,0},{8,4},{12,8},{16,12},{20,16},{24,20},{28,24},{32,28},{36,32}... | collective-permute-start | bytes 49160 | tf_op jit(solution)/shard_map/ppermute | solution.py:228
  24.7 1.9 %collective-permute-start = (bf16[16,512]{1,0:T(8,128)(2,1)S(1)}, bf16[16,512]{1,0:T(8,128)(2,1)S(1)}, u32[]{:S(2)}, u32[]{:S(2)}) collective-permute-start(bf16[16,512]{1,0:T(8,128)(2,1)S(1)} %get-tuple-element.34), channel_id=1, source_target_pairs={{0,4},{4,8},{8,12},{12,16},{16,20},{20,24},{24,28},{28,32},{32,36}... | collective-permute-start | bytes 49160 | tf_op jit(solution)/shard_map/ppermute | solution.py:227
  26.6 3.4 %collective-permute-done.1.after = bf16[16,512]{1,0:T(8,128)(2,1)S(1)} collective-permute-done((bf16[16,512]{1,0:T(8,128)(2,1)S(1)}, bf16[16,512]{1,0:T(8,128)(2,1)S(1)}, u32[]{:S(2)}, u32[]{:S(2)}) %collective-permute-start.1) | collective-permute-done | bytes 16416 | tf_op jit(solution)/shard_map/ppermute | solution.py:228
  30.0 1.9 %collective-permute-done.prev = bf16[16,512]{1,0:T(8,128)(2,1)S(1)} collective-permute-done((bf16[16,512]{1,0:T(8,128)(2,1)S(1)}, bf16[16,512]{1,0:T(8,128)(2,1)S(1)}, u32[]{:S(2)}, u32[]{:S(2)}) %collective-permute-start) | collective-permute-done | bytes 16416 | tf_op jit(solution)/shard_map/ppermute | solution.py:227
  31.9 5.9 %all-to-all-done.pieces = bf16[16,16,512]{2,1,0:T(8,128)(2,1)S(1)} async-done(((bf16[16,16,512]{2,1,0:T(8,128)(2,1)}), bf16[16,16,512]{2,1,0:T(8,128)(2,1)S(1)}, u32[]{:S(2)}, u32[]{:S(2)}) %all-to-all-start) | async-done | bytes 262176 | tf_op jit(solution)/shard_map/all_to_all | solution.py:236
  37.8 1.0 shard_map.75
  38.8 7.1 %all-to-all-start.1 = ((bf16[8,4,16,512]{3,2,1,0:T(8,128)(2,1)}), bf16[8,4,16,512]{3,2,1,0:T(8,128)(2,1)S(1)}, u32[]{:S(2)}, u32[]{:S(2)}) async-start(bf16[8,4,16,512]{3,2,1,0:T(8,128)(2,1)} %shard_map.75), calls=%async_computation.1 | async-start | bytes 1048576 | tf_op jit(solution)/shard_map/all_to_all | solution.py:245
  45.9 0.1 pad_add_fusion.info
  46.0 0.8 shard_map.74
  46.8 0.0 copy-start
  46.8 0.0 copy-start.2
  46.8 15.8 %all-to-all-done.1.in_own = bf16[8,4,16,512]{3,2,1,0:T(8,128)(2,1)S(1)} async-done(((bf16[8,4,16,512]{3,2,1,0:T(8,128)(2,1)}), bf16[8,4,16,512]{3,2,1,0:T(8,128)(2,1)S(1)}, u32[]{:S(2)}, u32[]{:S(2)}) %all-to-all-start.1) | async-done | bytes 524320 | tf_op jit(solution)/shard_map/all_to_all | solution.py:245
  62.6 35.2 %all_to_all.30.w_own = bf16[8,10,16,512]{3,2,1,0:T(8,128)(2,1)S(1)} all-to-all(bf16[8,10,16,512]{3,2,1,0:T(8,128)(2,1)S(1)} %shard_map.74), channel_id=1, replica_groups={{0,8,16,24,32,40,48,56},{4,12,20,28,36,44,52,60},{64,72,80,88,96,104,11..., dimensions={0} | all-to-all | bytes 2621440 | tf_op jit(solution)/shard_map/all_to_all | solution.py:248
  97.8 2.0 %collective-permute-start.9 = (bf16[8,10,16,512]{3,2,1,0:T(8,128)(2,1)S(1)}, bf16[8,10,16,512]{3,2,1,0:T(8,128)(2,1)S(1)}, u32[]{:S(2)}, u32[]{:S(2)}) collective-permute-start(bf16[8,10,16,512]{3,2,1,0:T(8,128)(2,1)S(1)} %all_to_all.30.w_own), channel_id=1, source_target_pairs={{0,4},{4,0},{8,12},{12,8},{16,20},{20,16},{24,28},{28,24},{32,36},... | collective-permute-start | bytes 3932168 | tf_op jit(solution)/shard_map/ppermute | solution.py:225
  99.9 2.4 %collective-permute-start.2 = (bf16[8,4,16,512]{3,2,1,0:T(8,128)(2,1)S(1)}, bf16[8,4,16,512]{3,2,1,0:T(8,128)(2,1)S(1)}, u32[]{:S(2)}, u32[]{:S(2)}) collective-permute-start(bf16[8,4,16,512]{3,2,1,0:T(8,128)(2,1)S(1)} %all-to-all-done.1.in_own), channel_id=1, source_target_pairs={{0,4},{4,0},{8,12},{12,8},{16,20},{20,16},{24,28},{28,24},{32,36},... | collective-permute-start | bytes 1572872 | tf_op jit(solution)/shard_map/ppermute | solution.py:225
  102.3 1.5 collective-permute-done.2.in_other
  103.8 0.0 copy-done
  103.8 0.0 copy-done.2
  103.8 1.3 shard_map.76
  105.1 4.9 %collective-permute-start.3 = (bf16[304,256]{1,0:T(8,128)(2,1)S(1)}, bf16[304,256]{1,0:T(8,128)(2,1)S(1)}, u32[]{:S(2)}, u32[]{:S(2)}) collective-permute-start(bf16[304,256]{1,0:T(8,128)(2,1)S(1)} %get-tuple-element.24), channel_id=1, source_target_pairs={{0,2},{1,3},{2,0},{3,1},{4,6},{5,7},{6,4},{7,5},{8,10},{9,11},{10,... | collective-permute-start | bytes 466952 | tf_op jit(solution)/shard_map/ppermute | solution.py:261
  110.1 2.5 %collective-permute-start.4 = (bf16[304,256]{1,0:T(8,128)(2,1)S(1)}, bf16[304,256]{1,0:T(8,128)(2,1)S(1)}, u32[]{:S(2)}, u32[]{:S(2)}) collective-permute-start(bf16[304,256]{1,0:T(8,128)(2,1)S(1)} %get-tuple-element.25), channel_id=1, source_target_pairs={{0,1},{1,2},{2,3},{3,0},{4,5},{5,6},{6,7},{7,4},{8,9},{9,10},{10,1... | collective-permute-start | bytes 466952 | tf_op jit(solution)/shard_map/ppermute | solution.py:261
  112.6 4.5 %collective-permute-start.5 = (bf16[304,256]{1,0:T(8,128)(2,1)S(1)}, bf16[304,256]{1,0:T(8,128)(2,1)S(1)}, u32[]{:S(2)}, u32[]{:S(2)}) collective-permute-start(bf16[304,256]{1,0:T(8,128)(2,1)S(1)} %get-tuple-element.26), channel_id=1, source_target_pairs={{0,3},{1,0},{2,1},{3,2},{4,7},{5,4},{6,5},{7,6},{8,11},{9,8},{10,9... | collective-permute-start | bytes 466952 | tf_op jit(solution)/shard_map/ppermute | solution.py:261
  117.1 0.0 collective-permute-done.3.refs_1_
  117.2 2.0 %collective-permute-done.4.refs_2_ = bf16[304,256]{1,0:T(8,128)(2,1)S(1)} collective-permute-done((bf16[304,256]{1,0:T(8,128)(2,1)S(1)}, bf16[304,256]{1,0:T(8,128)(2,1)S(1)}, u32[]{:S(2)}, u32[]{:S(2)}) %collective-permute-start.4) | collective-permute-done | bytes 155680 | tf_op jit(solution)/shard_map/ppermute | solution.py:261
  119.2 1.2 collective-permute-done.5.refs_3_
  120.4 0.0 copy-done.1
  120.4 1.3 shard_map.77.m_0
  121.7 5.6 %collective-permute-start.8 = (bf16[272,256]{1,0:T(8,128)(2,1)S(1)}, bf16[272,256]{1,0:T(8,128)(2,1)S(1)}, u32[]{:S(2)}, u32[]{:S(2)}) collective-permute-start(bf16[272,256]{1,0:T(8,128)(2,1)S(1)} %shard_map.77.m_0), channel_id=1, source_target_pairs={{0,3},{1,0},{2,1},{3,2},{4,7},{5,4},{6,5},{7,6},{8,11},{9,8},{10,9... | collective-permute-start | bytes 417800 | tf_op jit(solution)/shard_map/ppermute | solution.py:269
  127.3 1.9 %collective-permute-start.7 = (bf16[272,256]{1,0:T(8,128)(2,1)S(1)}, bf16[272,256]{1,0:T(8,128)(2,1)S(1)}, u32[]{:S(2)}, u32[]{:S(2)}) collective-permute-start(bf16[272,256]{1,0:T(8,128)(2,1)S(1)} %shard_map.77.m_0), channel_id=1, source_target_pairs={{0,2},{1,3},{2,0},{3,1},{4,6},{5,7},{6,4},{7,5},{8,10},{9,11},{10,... | collective-permute-start | bytes 417800 | tf_op jit(solution)/shard_map/ppermute | solution.py:269
  129.3 2.8 %collective-permute-start.6 = (bf16[272,256]{1,0:T(8,128)(2,1)S(1)}, bf16[272,256]{1,0:T(8,128)(2,1)S(1)}, u32[]{:S(2)}, u32[]{:S(2)}) collective-permute-start(bf16[272,256]{1,0:T(8,128)(2,1)S(1)} %shard_map.77.m_0), channel_id=1, source_target_pairs={{0,1},{1,2},{2,3},{3,0},{4,5},{5,6},{6,7},{7,4},{8,9},{9,10},{10,1... | collective-permute-start | bytes 417800 | tf_op jit(solution)/shard_map/ppermute | solution.py:269
  132.0 0.9 collective-permute-done.8.m_3
  132.9 4.1 %collective-permute-done.7.m_2 = bf16[272,256]{1,0:T(8,128)(2,1)S(1)} collective-permute-done((bf16[272,256]{1,0:T(8,128)(2,1)S(1)}, bf16[272,256]{1,0:T(8,128)(2,1)S(1)}, u32[]{:S(2)}, u32[]{:S(2)}) %collective-permute-start.7) | collective-permute-done | bytes 139296 | tf_op jit(solution)/shard_map/ppermute | solution.py:269
  137.0 1.1 collective-permute-done.6.m_1
  138.1 0.0 collective-permute-done.9.w_other
  138.1 2.6 %shard_map.78 = (bf16[272,512]{1,0:T(8,128)(2,1)S(1)}, bf16[4,288,256]{2,1,0:T(8,128)(2,1)}, bf16[2,8,2,16,512]{4,3,2,1,0:T(8,128)(2,1)S(1)}) custom-call(s32[4]{0:T(128)S(1)} %pad_add_fusion.info, bf16[16,512]{1,0:T(8,128)(2,1)S(1)} %collective-permute-done.prev, bf16[256,512]{1,0:T(8,128)(2,1)S(1)} %copy-done, ...), custom_call_target="tpu_custom_call" | custom-call | tf_op jit(solution)/shard_map/pallas_call | solution.py:208
  140.8 3.5 %all-to-all-start.3 = ((bf16[4,288,256]{2,1,0:T(8,128)(2,1)}), bf16[4,288,256]{2,1,0:T(8,128)(2,1)S(1)}, u32[]{:S(2)}, u32[]{:S(2)}) async-start(bf16[4,288,256]{2,1,0:T(8,128)(2,1)} %get-tuple-element.29), calls=%async_computation.3 | async-start | bytes 1179648 | tf_op jit(solution)/shard_map/all_to_all | solution.py:252
  144.2 1.9 %collective-permute-start.10 = (bf16[2,8,2,16,512]{4,3,2,1,0:T(8,128)(2,1)S(1)}, bf16[2,8,2,16,512]{4,3,2,1,0:T(8,128)(2,1)S(1)}, u32[]{:S(2)}, u32[]{:S(2)}) collective-permute-start(bf16[2,8,2,16,512]{4,3,2,1,0:T(8,128)(2,1)S(1)} %get-tuple-element.30.half), channel_id=1, source_target_pairs={{0,64},{4,68},{8,72},{12,76},{16,80},{20,84},{24,88},{28,92},{32,9... | collective-permute-start | bytes 1572872 | tf_op jit(solution)/shard_map/ppermute | solution.py:280
  146.2 6.7 %all-to-all-done.3.refs_0_ = bf16[4,288,256]{2,1,0:T(8,128)(2,1)S(1)} async-done(((bf16[4,288,256]{2,1,0:T(8,128)(2,1)}), bf16[4,288,256]{2,1,0:T(8,128)(2,1)S(1)}, u32[]{:S(2)}, u32[]{:S(2)}) %all-to-all-start.3) | async-done | bytes 589856 | tf_op jit(solution)/shard_map/all_to_all | solution.py:252
  152.8 2.1 %shard_map.79 = bf16[4,256,256]{2,1,0:T(8,128)(2,1)} custom-call(s32[4]{0:T(128)S(1)} %pad_add_fusion.info, bf16[2,1,256,256]{3,2,1,0:T(8,128)(2,1)S(1)} %copy-done.1, f32[2,256]{1,0:T(2,128)S(1)} %copy-done.3, bf16[4,288,256]{2,1,0:T(8,128)(2,1)S(1)} %all-to-all-done.3.refs_0_), custom_call_target="tpu_custom_call" | custom-call | tf_op jit(solution)/shard_map/pallas_call | solution.py:208
  154.9 3.6 %all-to-all-start.4 = ((bf16[4,256,256]{2,1,0:T(8,128)(2,1)}), bf16[4,256,256]{2,1,0:T(8,128)(2,1)S(1)}, u32[]{:S(2)}, u32[]{:S(2)}) async-start(bf16[4,256,256]{2,1,0:T(8,128)(2,1)} %shard_map.79), calls=%async_computation.4 | async-start | bytes 1048576 | tf_op jit(solution)/shard_map/all_to_all | solution.py:252
  158.5 0.0 collective-permute-done.10.other_half
  158.5 8.0 %all-to-all-done.4.mixed = bf16[4,256,256]{2,1,0:T(8,128)(2,1)S(1)} async-done(((bf16[4,256,256]{2,1,0:T(8,128)(2,1)}), bf16[4,256,256]{2,1,0:T(8,128)(2,1)S(1)}, u32[]{:S(2)}, u32[]{:S(2)}) %all-to-all-start.4) | async-done | bytes 524320 | tf_op jit(solution)/shard_map/all_to_all | solution.py:252
  166.6 1.3 shard_map.80
  167.9 7.8 %all_to_all.31.squares = f32[4,8,256]{2,1,0:T(8,128)S(1)} all-to-all(f32[4,8,256]{2,1,0:T(8,128)S(1)} %get-tuple-element.32), channel_id=1, replica_groups=mesh['sp'=256,'tp'=4] {'tp'}, dimensions={0} | all-to-all | bytes 65536 | tf_op jit(solution)/shard_map/all_to_all | solution.py:252
  175.7 0.9 shard_map.81
  (5 shorter events, 0.0 us)
Async XLA Ops:
  1.4 36.3 %all-to-all-start = ((bf16[16,16,512]{2,1,0:T(8,128)(2,1)}), bf16[16,16,512]{2,1,0:T(8,128)(2,1)S(1)}, u32[]{:S(2)}, u32[]{:S(2)}) async-start(bf16[16,16,512]{2,1,0:T(8,128)(2,1)} %shard_map.73), calls=%async_computation | async-start | bytes 524288 | tf_op jit(solution)/shard_map/all_to_all | solution.py:236
  20.6 9.4 %collective-permute-start.1 = (bf16[16,512]{1,0:T(8,128)(2,1)S(1)}, bf16[16,512]{1,0:T(8,128)(2,1)S(1)}, u32[]{:S(2)}, u32[]{:S(2)}) collective-permute-start(bf16[16,512]{1,0:T(8,128)(2,1)S(1)} %get-tuple-element.33), channel_id=1, source_target_pairs={{4,0},{8,4},{12,8},{16,12},{20,16},{24,20},{28,24},{32,28},{36,32}... | collective-permute-start | bytes 49160 | tf_op jit(solution)/shard_map/ppermute | solution.py:228
  24.7 7.2 %collective-permute-start = (bf16[16,512]{1,0:T(8,128)(2,1)S(1)}, bf16[16,512]{1,0:T(8,128)(2,1)S(1)}, u32[]{:S(2)}, u32[]{:S(2)}) collective-permute-start(bf16[16,512]{1,0:T(8,128)(2,1)S(1)} %get-tuple-element.34), channel_id=1, source_target_pairs={{0,4},{4,8},{8,12},{12,16},{16,20},{20,24},{24,28},{28,32},{32,36}... | collective-permute-start | bytes 49160 | tf_op jit(solution)/shard_map/ppermute | solution.py:227
  38.8 23.8 %all-to-all-start.1 = ((bf16[8,4,16,512]{3,2,1,0:T(8,128)(2,1)}), bf16[8,4,16,512]{3,2,1,0:T(8,128)(2,1)S(1)}, u32[]{:S(2)}, u32[]{:S(2)}) async-start(bf16[8,4,16,512]{3,2,1,0:T(8,128)(2,1)} %shard_map.75), calls=%async_computation.1 | async-start | bytes 1048576 | tf_op jit(solution)/shard_map/all_to_all | solution.py:245
  46.8 57.0 %copy-start = (bf16[256,512]{1,0:T(8,128)(2,1)S(1)}, bf16[256,512]{1,0:T(8,128)(2,1)}, u32[]{:S(2)}) copy-start(bf16[256,512]{1,0:T(8,128)(2,1)} %own.3) | copy-start | bytes 786436
  46.8 57.0 %copy-start.2 = (f32[2,512]{1,0:T(2,128)S(1)}, f32[2,512]{1,0:T(2,128)}, u32[]{:S(2)}) copy-start(f32[2,512]{1,0:T(2,128)} %gain.3) | copy-start | bytes 12292
  97.8 22.6 %copy-start.1 = (bf16[2,1,256,256]{3,2,1,0:T(8,128)(2,1)S(1)}, bf16[2,1,256,256]{3,2,1,0:T(8,128)(2,1)}, u32[]{:S(2)}) copy-start(bf16[2,1,256,256]{3,2,1,0:T(8,128)(2,1)} %wp.3) | copy-start | bytes 786436
  97.8 22.6 %copy-start.3 = (f32[2,256]{1,0:T(2,128)S(1)}, f32[2,256]{1,0:T(2,128)}, u32[]{:S(2)}) copy-start(f32[2,256]{1,0:T(2,128)} %scale.3) | copy-start | bytes 6148
  97.8 40.3 %collective-permute-start.9 = (bf16[8,10,16,512]{3,2,1,0:T(8,128)(2,1)S(1)}, bf16[8,10,16,512]{3,2,1,0:T(8,128)(2,1)S(1)}, u32[]{:S(2)}, u32[]{:S(2)}) collective-permute-start(bf16[8,10,16,512]{3,2,1,0:T(8,128)(2,1)S(1)} %all_to_all.30.w_own), channel_id=1, source_target_pairs={{0,4},{4,0},{8,12},{12,8},{16,20},{20,16},{24,28},{28,24},{32,36},... | collective-permute-start | bytes 3932168 | tf_op jit(solution)/shard_map/ppermute | solution.py:225
  99.9 3.9 %collective-permute-start.2 = (bf16[8,4,16,512]{3,2,1,0:T(8,128)(2,1)S(1)}, bf16[8,4,16,512]{3,2,1,0:T(8,128)(2,1)S(1)}, u32[]{:S(2)}, u32[]{:S(2)}) collective-permute-start(bf16[8,4,16,512]{3,2,1,0:T(8,128)(2,1)S(1)} %all-to-all-done.1.in_own), channel_id=1, source_target_pairs={{0,4},{4,0},{8,12},{12,8},{16,20},{20,16},{24,28},{28,24},{32,36},... | collective-permute-start | bytes 1572872 | tf_op jit(solution)/shard_map/ppermute | solution.py:225
  105.1 12.0 %collective-permute-start.3 = (bf16[304,256]{1,0:T(8,128)(2,1)S(1)}, bf16[304,256]{1,0:T(8,128)(2,1)S(1)}, u32[]{:S(2)}, u32[]{:S(2)}) collective-permute-start(bf16[304,256]{1,0:T(8,128)(2,1)S(1)} %get-tuple-element.24), channel_id=1, source_target_pairs={{0,2},{1,3},{2,0},{3,1},{4,6},{5,7},{6,4},{7,5},{8,10},{9,11},{10,... | collective-permute-start | bytes 466952 | tf_op jit(solution)/shard_map/ppermute | solution.py:261
  110.1 9.1 %collective-permute-start.4 = (bf16[304,256]{1,0:T(8,128)(2,1)S(1)}, bf16[304,256]{1,0:T(8,128)(2,1)S(1)}, u32[]{:S(2)}, u32[]{:S(2)}) collective-permute-start(bf16[304,256]{1,0:T(8,128)(2,1)S(1)} %get-tuple-element.25), channel_id=1, source_target_pairs={{0,1},{1,2},{2,3},{3,0},{4,5},{5,6},{6,7},{7,4},{8,9},{9,10},{10,1... | collective-permute-start | bytes 466952 | tf_op jit(solution)/shard_map/ppermute | solution.py:261
  112.6 7.8 %collective-permute-start.5 = (bf16[304,256]{1,0:T(8,128)(2,1)S(1)}, bf16[304,256]{1,0:T(8,128)(2,1)S(1)}, u32[]{:S(2)}, u32[]{:S(2)}) collective-permute-start(bf16[304,256]{1,0:T(8,128)(2,1)S(1)} %get-tuple-element.26), channel_id=1, source_target_pairs={{0,3},{1,0},{2,1},{3,2},{4,7},{5,4},{6,5},{7,6},{8,11},{9,8},{10,9... | collective-permute-start | bytes 466952 | tf_op jit(solution)/shard_map/ppermute | solution.py:261
  121.7 11.2 %collective-permute-start.8 = (bf16[272,256]{1,0:T(8,128)(2,1)S(1)}, bf16[272,256]{1,0:T(8,128)(2,1)S(1)}, u32[]{:S(2)}, u32[]{:S(2)}) collective-permute-start(bf16[272,256]{1,0:T(8,128)(2,1)S(1)} %shard_map.77.m_0), channel_id=1, source_target_pairs={{0,3},{1,0},{2,1},{3,2},{4,7},{5,4},{6,5},{7,6},{8,11},{9,8},{10,9... | collective-permute-start | bytes 417800 | tf_op jit(solution)/shard_map/ppermute | solution.py:269
  127.3 9.7 %collective-permute-start.7 = (bf16[272,256]{1,0:T(8,128)(2,1)S(1)}, bf16[272,256]{1,0:T(8,128)(2,1)S(1)}, u32[]{:S(2)}, u32[]{:S(2)}) collective-permute-start(bf16[272,256]{1,0:T(8,128)(2,1)S(1)} %shard_map.77.m_0), channel_id=1, source_target_pairs={{0,2},{1,3},{2,0},{3,1},{4,6},{5,7},{6,4},{7,5},{8,10},{9,11},{10,... | collective-permute-start | bytes 417800 | tf_op jit(solution)/shard_map/ppermute | solution.py:269
  129.3 8.9 %collective-permute-start.6 = (bf16[272,256]{1,0:T(8,128)(2,1)S(1)}, bf16[272,256]{1,0:T(8,128)(2,1)S(1)}, u32[]{:S(2)}, u32[]{:S(2)}) collective-permute-start(bf16[272,256]{1,0:T(8,128)(2,1)S(1)} %shard_map.77.m_0), channel_id=1, source_target_pairs={{0,1},{1,2},{2,3},{3,0},{4,5},{5,6},{6,7},{7,4},{8,9},{9,10},{10,1... | collective-permute-start | bytes 417800 | tf_op jit(solution)/shard_map/ppermute | solution.py:269
  140.8 12.1 %all-to-all-start.3 = ((bf16[4,288,256]{2,1,0:T(8,128)(2,1)}), bf16[4,288,256]{2,1,0:T(8,128)(2,1)S(1)}, u32[]{:S(2)}, u32[]{:S(2)}) async-start(bf16[4,288,256]{2,1,0:T(8,128)(2,1)} %get-tuple-element.29), calls=%async_computation.3 | async-start | bytes 1179648 | tf_op jit(solution)/shard_map/all_to_all | solution.py:252
  144.2 14.3 %collective-permute-start.10 = (bf16[2,8,2,16,512]{4,3,2,1,0:T(8,128)(2,1)S(1)}, bf16[2,8,2,16,512]{4,3,2,1,0:T(8,128)(2,1)S(1)}, u32[]{:S(2)}, u32[]{:S(2)}) collective-permute-start(bf16[2,8,2,16,512]{4,3,2,1,0:T(8,128)(2,1)S(1)} %get-tuple-element.30.half), channel_id=1, source_target_pairs={{0,64},{4,68},{8,72},{12,76},{16,80},{20,84},{24,88},{28,92},{32,9... | collective-permute-start | bytes 1572872 | tf_op jit(solution)/shard_map/ppermute | solution.py:280
  154.9 20.8 %copy-start.4 = (f32[512]{0:T(512)S(1)}, f32[512]{0:T(512)}, u32[]{:S(2)}) copy-start(f32[512]{0:T(512)} %param.13) | copy-start | bytes 6148
  154.9 11.7 %all-to-all-start.4 = ((bf16[4,256,256]{2,1,0:T(8,128)(2,1)}), bf16[4,256,256]{2,1,0:T(8,128)(2,1)S(1)}, u32[]{:S(2)}, u32[]{:S(2)}) async-start(bf16[4,256,256]{2,1,0:T(8,128)(2,1)} %shard_map.79), calls=%async_computation.4 | async-start | bytes 1048576 | tf_op jit(solution)/shard_map/all_to_all | solution.py:252
